TPU v7x, 512 devices: a whole 4x8x8 slice. The times are simulated.
512 devices in a mesh: ep: 128 (over z, y, core), tp: 4 (over x).
Axes of the slice: x: 4, y: 8, z: 8, core: 2. Of those that a mesh axis runs over, the one named last changes fastest.
Arguments:
- tokens: bfloat16 [8192, 1024], P('ep', 'tp'), may hold values from -6 to 6
- conv_state: bfloat16 [8192, 3, 512], P('ep', None, 'tp'), may hold values from -6 to 6
- lru_state: float32 [8192, 512], P('ep', 'tp'), may hold values from -6 to 6
- mix_gain: bfloat16 [1024], replicated, may hold values from 0.099609375 to 1.8984375
- ffn_gain: bfloat16 [1024], replicated, may hold values from 0.099609375 to 1.8984375
- w_branch: bfloat16 [1024, 512], P(None, 'tp'), may hold values from -0.1875 to 0.1875
- w_gate: bfloat16 [1024, 512], P(None, 'tp'), may hold values from -0.1875 to 0.1875
- conv_taps: bfloat16 [4, 512], P(None, 'tp'), may hold values from -3 to 3
- w_recur: bfloat16 [8, 64, 64], P('tp'), may hold values from -0.75 to 0.75
- w_inject: bfloat16 [8, 64, 64], P('tp'), may hold values from -0.75 to 0.75
- lru_lambda: float32 [512], P('tp'), may hold values from 2 to 7
- w_out: bfloat16 [512, 1024], P('tp'), may hold values from -0.25 to 0.25
- expert_gate: bfloat16 [128, 1024, 2560], P('ep', None, 'tp'), may hold values from -0.1875 to 0.1875
- expert_up: bfloat16 [128, 1024, 2560], P('ep', None, 'tp'), may hold values from -0.1875 to 0.1875
- expert_down: bfloat16 [128, 2560, 1024], P('ep', 'tp'), may hold values from -0.125 to 0.125
- route_ids: int32 [8192, 2], P('ep'), may hold values from 0 to 127, all different within a row; in each aligned block of 64 rows (0 to 63, 64 to 127, ...) at most 2 rows name the same one
- route_weight: float32 [8192, 2], P('ep'), may hold values from 0.2 to 1
Outputs:
- mixed: bfloat16 [8192, 1024], P('ep', 'tp')
- state_out: float32 [8192, 512], P('ep', 'tp')
Inputs may be any that keep to these rules, and one draw needn't show every extreme that they name: `route_ids`: each row names 2 different experts. Among the 64 rows of one device no expert is named more than 2 times, and in every draw some expert is named exactly 2 times by them.
All inputs are finite; a program needn't handle non-finite values.
Results may differ from a plain program's by a relative error of at most 0.015.
Values may be sent and summed in bfloat16 or wider, within the bound.
A program may use at most 64 MiB of HBM per device.

v0:
```python
import jax
import jax.numpy as jnp
from jax import lax
from jax.sharding import PartitionSpec as P

EPS = 1e-06
LRU_SCALE = 8.0


def joined_along(pieces, dim):
    pieces = jnp.moveaxis(pieces, 0, dim)
    lengths = pieces.shape
    return pieces.reshape(*lengths[:dim], lengths[dim] * lengths[dim + 1], *lengths[dim + 2 :])


def sent_to_all(x, axis):
    count = lax.axis_size(axis)
    return lax.all_to_all(jnp.broadcast_to(x[None], (count, *x.shape)), axis, 0, 0, tiled=True)


def gathered_copies(x, axis, dim):
    return joined_along(sent_to_all(x, axis), dim)


def in_blocks(x, dim, count):
    lengths = x.shape
    pieces = x.reshape(*lengths[:dim], count, lengths[dim] // count, *lengths[dim + 1 :])
    return jnp.moveaxis(pieces, dim, 0)


def sent_and_summed(x, axis, dim):
    pieces = in_blocks(x, dim, lax.axis_size(axis))
    arrived = lax.all_to_all(pieces, axis, split_axis=0, concat_axis=0, tiled=True)
    return arrived.astype(jnp.float32).sum(axis=0)


def rms_rows(rows, gain):
    values = rows.astype(jnp.float32)
    scaled = values * lax.rsqrt(jnp.mean(values * values, axis=-1, keepdims=True) + EPS)
    return (scaled * gain.astype(jnp.float32)).astype(jnp.bfloat16)


def body(
    tokens,
    conv_state,
    lru_state,
    mix_gain,
    ffn_gain,
    w_branch,
    w_gate,
    conv_taps,
    w_recur,
    w_inject,
    lru_lambda,
    w_out,
    expert_gate,
    expert_up,
    expert_down,
    route_ids,
    route_weight,
):
    seqs = tokens.shape[0]
    whole = gathered_copies(tokens, "tp", 1)
    normed = rms_rows(whole, mix_gain)
    branch = jnp.dot(normed, w_branch, preferred_element_type=jnp.float32).astype(jnp.bfloat16)
    gate_in = jnp.dot(normed, w_gate, preferred_element_type=jnp.float32).astype(jnp.bfloat16)
    window = jnp.concatenate([conv_state, branch[:, None, :]], axis=1).astype(jnp.float32)
    conv_out = jnp.sum(window * conv_taps.astype(jnp.float32)[None], axis=1)
    heads_here = w_recur.shape[0]
    head_width = w_recur.shape[1]
    conv_heads = conv_out.astype(jnp.bfloat16).reshape(seqs, heads_here, head_width)
    recur = jax.nn.sigmoid(
        jnp.einsum("nhi,hij->nhj", conv_heads, w_recur, preferred_element_type=jnp.float32).reshape(
            seqs, -1
        )
    )
    inject = jax.nn.sigmoid(
        jnp.einsum(
            "nhi,hij->nhj", conv_heads, w_inject, preferred_element_type=jnp.float32
        ).reshape(seqs, -1)
    )
    log_decay = -LRU_SCALE * recur * jax.nn.softplus(-lru_lambda)
    state_out = (
        jnp.exp(log_decay) * lru_state + jnp.sqrt(-jnp.expm1(2.0 * log_decay)) * inject * conv_out
    )
    lru_out = (state_out * jax.nn.gelu(gate_in.astype(jnp.float32))).astype(jnp.bfloat16)
    partial_value = jnp.dot(lru_out, w_out, preferred_element_type=jnp.float32)
    partial_value = lax.optimization_barrier(partial_value.astype(jnp.bfloat16)).astype(jnp.float32)
    mix_out = sent_and_summed(partial_value.astype(jnp.bfloat16), "tp", 1).astype(jnp.bfloat16)
    resid = (tokens.astype(jnp.float32) + mix_out.astype(jnp.float32)).astype(jnp.bfloat16)
    top = route_ids.shape[1]
    local = expert_gate.shape[0]
    experts = lax.axis_size("ep") * local
    capacity = max(2, 2 * seqs * top // experts)
    flat = route_ids.reshape(-1)
    onehot = (flat[:, None] == jnp.arange(experts, dtype=jnp.int32)[None, :]).astype(jnp.int32)
    before = jnp.cumsum(onehot, axis=0) - onehot
    slot = jnp.sum(before * onehot, axis=1)
    slot_id = slot * experts + flat
    places = jnp.arange(capacity * experts, dtype=jnp.int32)
    hits = slot_id[None, :] == places[:, None]
    dispatch = jnp.sum(
        hits.reshape(capacity * experts, seqs, top).astype(jnp.float32), axis=2
    ).astype(jnp.bfloat16)
    spread = jnp.transpose(hits).reshape(seqs, top, capacity * experts)
    combine = jnp.sum(jnp.where(spread, route_weight[:, :, None], 0.0), axis=1)
    full = gathered_copies(resid, "tp", 1)
    normed2 = rms_rows(full, ffn_gain)
    buffer = jnp.dot(dispatch, normed2, preferred_element_type=jnp.float32).astype(jnp.bfloat16)
    buffer = buffer.reshape(capacity, experts, -1)
    block = lax.all_to_all(buffer, "ep", split_axis=1, concat_axis=1, tiled=True)
    count = block.shape[0]
    width = block.shape[2]
    grid = block.reshape(count, -1, local, width)
    rows = grid[:, :, 0].reshape(-1, width)
    first = jnp.dot(rows, expert_gate[0], preferred_element_type=jnp.float32)
    second = jnp.dot(rows, expert_up[0], preferred_element_type=jnp.float32)
    hidden = (jax.nn.silu(first) * second).astype(jnp.bfloat16)
    term = jnp.dot(hidden, expert_down[0], preferred_element_type=jnp.float32)
    term = lax.optimization_barrier(term.astype(jnp.bfloat16)).astype(jnp.float32)
    summed = sent_and_summed(term.astype(jnp.bfloat16), "tp", 1).astype(jnp.bfloat16)
    results = summed.reshape(count, -1, 1, summed.shape[1])
    answered = results.reshape(count, -1, results.shape[3])
    returned = lax.all_to_all(answered, "ep", split_axis=1, concat_axis=1, tiled=True)
    back = returned.reshape(capacity * experts, -1).astype(jnp.float32)
    moe = jnp.dot(combine, back)
    mixed = (resid.astype(jnp.float32) + moe).astype(jnp.bfloat16)
    return (mixed, state_out)


def solution(mesh):
    placed = (
        P("ep", "tp"),
        P("ep", None, "tp"),
        P("ep", "tp"),
        P(),
        P(),
        P(None, "tp"),
        P(None, "tp"),
        P(None, "tp"),
        P("tp", None, None),
        P("tp", None, None),
        P("tp"),
        P("tp", None),
        P("ep", None, "tp"),
        P("ep", None, "tp"),
        P("ep", "tp", None),
        P("ep", None),
        P("ep", None),
    )
    return jax.shard_map(
        body, mesh=mesh, in_specs=placed, out_specs=(P("ep", "tp"), P("ep", "tp")), check_vma=False
    )
```

profile of v0, /device:TPU:1, one launch (start us, length us, event | category | flops | bytes accessed | tf_op | source)
XLA Modules:
  0.0 109.8 jit_solution(5886516992850330418)
XLA Ops:
  0.7 1.5 %broadcast_in_dim.14 = bf16[4,64,256]{2,1,0:T(8,128)(2,1)} broadcast(bf16[64,256]{1,0:T(8,128)(2,1)} %param.17), dimensions={1,2} | broadcast | bytes 163840 | tf_op jit(solution)/shard_map/broadcast_in_dim | solution.py:18
  2.2 4.8 %all-to-all-start = ((bf16[4,64,256]{2,1,0:T(8,128)(2,1)}), bf16[4,64,256]{2,1,0:T(8,128)(2,1)S(1)}, u32[]{:S(2)}, u32[]{:S(2)}) async-start(bf16[4,64,256]{2,1,0:T(8,128)(2,1)} %broadcast_in_dim.14), calls=%async_computation | async-start | bytes 262144 | tf_op jit(solution)/shard_map/all_to_all | solution.py:18
  7.0 0.7 convert_element_type.113
  7.7 0.7 convert_element_type.117
  8.4 0.7 fusion.55
  9.1 0.8 copy.80
  10.4 1.4 %all-to-all-done = bf16[4,64,256]{2,1,0:T(8,128)(2,1)S(1)} async-done(((bf16[4,64,256]{2,1,0:T(8,128)(2,1)}), bf16[4,64,256]{2,1,0:T(8,128)(2,1)S(1)}, u32[]{:S(2)}, u32[]{:S(2)}) %all-to-all-start) | async-done | bytes 131104 | tf_op jit(solution)/shard_map/all_to_all | solution.py:18
  13.2 0.4 convolution_convert_fusion.1
  13.6 0.6 copy.99
  14.3 3.3 %all-to-all-start.1 = ((bf16[4,64,256]{2,1,0:T(8,128)(2,1)}), bf16[4,64,256]{2,1,0:T(8,128)(2,1)S(1)}, u32[]{:S(2)}, u32[]{:S(2)}) async-start(bf16[4,64,256]{2,1,0:T(8,128)(2,1)} %bitcast.58), calls=%async_computation.1 | async-start | bytes 262144 | tf_op jit(solution)/shard_map/all_to_all | solution.py:33
  17.8 4.5 %all-to-all-done.1 = bf16[4,64,256]{2,1,0:T(8,128)(2,1)S(1)} async-done(((bf16[4,64,256]{2,1,0:T(8,128)(2,1)}), bf16[4,64,256]{2,1,0:T(8,128)(2,1)S(1)}, u32[]{:S(2)}, u32[]{:S(2)}) %all-to-all-start.1) | async-done | bytes 131104 | tf_op jit(solution)/shard_map/all_to_all | solution.py:33
  22.4 0.6 broadcast_in_dim.22
  23.1 3.3 %all-to-all-start.2 = ((bf16[4,64,256]{2,1,0:T(8,128)(2,1)}), bf16[4,64,256]{2,1,0:T(8,128)(2,1)S(1)}, u32[]{:S(2)}, u32[]{:S(2)}) async-start(bf16[4,64,256]{2,1,0:T(8,128)(2,1)} %broadcast_in_dim.22), calls=%async_computation.2 | async-start | bytes 262144 | tf_op jit(solution)/shard_map/all_to_all | solution.py:18
  26.5 4.7 %all-to-all-done.2 = bf16[4,64,256]{2,1,0:T(8,128)(2,1)S(1)} async-done(((bf16[4,64,256]{2,1,0:T(8,128)(2,1)}), bf16[4,64,256]{2,1,0:T(8,128)(2,1)S(1)}, u32[]{:S(2)}, u32[]{:S(2)}) %all-to-all-start.2) | async-done | bytes 131104 | tf_op jit(solution)/shard_map/all_to_all | solution.py:18
  31.4 0.4 convolution_convert_fusion
  31.8 0.5 copy.83
  32.3 41.8 %all_to_all.30 = bf16[2,128,1024]{2,0,1:T(2,128)(2,1)S(1)} all-to-all(bf16[2,128,1024]{2,0,1:T(2,128)(2,1)S(1)} %copy.83), channel_id=1, replica_groups=mesh['ep'=128,'tp'=4] {'ep'}, dimensions={1} | all-to-all | bytes 1048576 | tf_op jit(solution)/shard_map/all_to_all | solution.py:111
  74.3 0.6 fusion.4
  74.9 2.4 %fusion.6 = bf16[256,1024]{1,0:T(8,128)(2,1)S(1)} fusion(bf16[1,640,1024]{2,1,0:T(8,128)(2,1)S(1)} %copy-done, bf16[256,1024]{1,0:T(8,128)(2,1)S(1)} %bitcast.62, bf16[1,1024,640]{2,1,0:T(8,128)(2,1)} %param.30, f32[256,640]{1,0:T(8,128)S(1)} %fusion.4), kind=kOutput, calls=%fused_computation.6 | convolution fusion | flops 672333824 | bytes 4325376 | tf_op jit(solution)/shard_map/dot_general | solution.py:119
  77.3 12.2 %all_to_all.31 = bf16[4,256,256]{2,1,0:T(8,128)(2,1)S(1)} all-to-all(bf16[4,256,256]{2,1,0:T(8,128)(2,1)S(1)} %bitcast.64), channel_id=1, replica_groups=mesh['ep'=128,'tp'=4] {'tp'}, dimensions={0} | all-to-all | bytes 1048576 | tf_op jit(solution)/shard_map/all_to_all | solution.py:33
  89.6 0.8 copy.86
  90.4 5.8 %all-to-all-start.5 = ((bf16[2,128,256]{2,0,1:T(2,128)(2,1)}), bf16[2,128,256]{2,0,1:T(2,128)(2,1)S(1)}, u32[]{:S(2)}, u32[]{:S(2)}) async-start(bf16[2,128,256]{2,0,1:T(2,128)(2,1)} %copy.86), calls=%async_computation.5 | async-start | bytes 262144 | tf_op jit(solution)/shard_map/all_to_all | solution.py:124
  96.3 12.7 %all-to-all-done.5 = bf16[2,128,256]{2,0,1:T(2,128)(2,1)S(1)} async-done(((bf16[2,128,256]{2,0,1:T(2,128)(2,1)}), bf16[2,128,256]{2,0,1:T(2,128)(2,1)S(1)}, u32[]{:S(2)}, u32[]{:S(2)}) %all-to-all-start.5) | async-done | bytes 131104 | tf_op jit(solution)/shard_map/all_to_all | solution.py:124
  109.0 0.8 fusion.25
  (64 shorter events, 2.7 us)
Async XLA Ops:
  0.6 74.2 %copy-start = (bf16[1,640,1024]{2,1,0:T(8,128)(2,1)S(1)}, bf16[1,640,1024]{2,1,0:T(8,128)(2,1)}, u32[]{:S(2)}) copy-start(bf16[1,640,1024]{2,1,0:T(8,128)(2,1)} %param.31) | copy-start | bytes 3932164
  0.6 11.4 %copy-start.4 = (bf16[1024,128]{1,0:T(8,128)(2,1)S(1)}, bf16[1024,128]{1,0:T(8,128)(2,1)}, u32[]{:S(2)}) copy-start(bf16[1024,128]{1,0:T(8,128)(2,1)} %param.22) | copy-start | bytes 786436
  0.7 11.7 %copy-start.7 = (bf16[64,3,128]{2,0,1:T(8,128)(2,1)S(1)}, bf16[64,3,128]{2,0,1:T(8,128)(2,1)}, u32[]{:S(2)}) copy-start(bf16[64,3,128]{2,0,1:T(8,128)(2,1)} %param.18) | copy-start | bytes 147460
  0.7 11.8 %copy-start.12 = (bf16[2,64,64]{2,1,0:T(8,128)(2,1)S(1)}, bf16[2,64,64]{2,1,0:T(8,128)(2,1)}, u32[]{:S(2)}) copy-start(bf16[2,64,64]{2,1,0:T(8,128)(2,1)} %param.25) | copy-start | bytes 49156
  2.2 9.7 %all-to-all-start = ((bf16[4,64,256]{2,1,0:T(8,128)(2,1)}), bf16[4,64,256]{2,1,0:T(8,128)(2,1)S(1)}, u32[]{:S(2)}, u32[]{:S(2)}) async-start(bf16[4,64,256]{2,1,0:T(8,128)(2,1)} %broadcast_in_dim.14), calls=%async_computation | async-start | bytes 262144 | tf_op jit(solution)/shard_map/all_to_all | solution.py:18
  10.0 2.8 %copy-start.13 = (bf16[2,64,64]{2,1,0:T(8,128)(2,1)S(1)}, bf16[2,64,64]{2,1,0:T(8,128)(2,1)}, u32[]{:S(2)}) copy-start(bf16[2,64,64]{2,1,0:T(8,128)(2,1)} %param.26) | copy-start | bytes 49156
  11.9 1.3 %copy-start.8 = (f32[64,128]{1,0:T(8,128)S(1)}, f32[64,128]{1,0:T(8,128)}, u32[]{:S(2)}) copy-start(f32[64,128]{1,0:T(8,128)} %param.19) | copy-start | bytes 98308
  11.9 1.3 %copy-start.2 = (bf16[128,1024]{1,0:T(8,128)(2,1)S(1)}, bf16[128,1024]{1,0:T(8,128)(2,1)}, u32[]{:S(2)}) copy-start(bf16[128,1024]{1,0:T(8,128)(2,1)} %param.28) | copy-start | bytes 786436
  11.9 1.3 %copy-start.3 = (bf16[1024,128]{1,0:T(8,128)(2,1)S(1)}, bf16[1024,128]{1,0:T(8,128)(2,1)}, u32[]{:S(2)}) copy-start(bf16[1024,128]{1,0:T(8,128)(2,1)} %param.23) | copy-start | bytes 786436
  12.6 5.2 %copy-start.9 = (s32[64,2]{0,1:T(2,128)S(1)}, s32[64,2]{0,1:T(2,128)}, u32[]{:S(2)}) copy-start(s32[64,2]{0,1:T(2,128)} %param.32) | copy-start | bytes 1540
  12.6 5.2 %copy-start.10 = (bf16[1024]{0:T(1024)(128)(2,1)S(1)}, bf16[1024]{0:T(1024)(128)(2,1)}, u32[]{:S(2)}) copy-start(bf16[1024]{0:T(1024)(128)(2,1)} %param.21) | copy-start | bytes 6148
  12.6 9.8 %copy-start.5 = (bf16[64,256]{1,0:T(8,128)(2,1)S(1)}, bf16[64,256]{1,0:T(8,128)(2,1)}, u32[]{:S(2)}) copy-start(bf16[64,256]{1,0:T(8,128)(2,1)} %param.17) | copy-start | bytes 98308
  13.2 18.0 %copy-start.6 = (f32[64,128]{1,0:T(8,128)}, f32[64,128]{1,0:T(8,128)S(1)}, u32[]{:S(2)}) copy-start(f32[64,128]{1,0:T(8,128)S(1)} %multiply_add_fusion) | copy-start | bytes 98308
  14.3 8.1 %all-to-all-start.1 = ((bf16[4,64,256]{2,1,0:T(8,128)(2,1)}), bf16[4,64,256]{2,1,0:T(8,128)(2,1)S(1)}, u32[]{:S(2)}, u32[]{:S(2)}) async-start(bf16[4,64,256]{2,1,0:T(8,128)(2,1)} %bitcast.58), calls=%async_computation.1 | async-start | bytes 262144 | tf_op jit(solution)/shard_map/all_to_all | solution.py:33
  23.1 8.1 %all-to-all-start.2 = ((bf16[4,64,256]{2,1,0:T(8,128)(2,1)}), bf16[4,64,256]{2,1,0:T(8,128)(2,1)S(1)}, u32[]{:S(2)}, u32[]{:S(2)}) async-start(bf16[4,64,256]{2,1,0:T(8,128)(2,1)} %broadcast_in_dim.22), calls=%async_computation.2 | async-start | bytes 262144 | tf_op jit(solution)/shard_map/all_to_all | solution.py:18
  32.3 41.9 %copy-start.1 = (bf16[1,1024,640]{2,1,0:T(8,128)(2,1)S(1)}, bf16[1,1024,640]{2,1,0:T(8,128)(2,1)}, u32[]{:S(2)}) copy-start(bf16[1,1024,640]{2,1,0:T(8,128)(2,1)} %param.29) | copy-start | bytes 3932164
  77.3 18.9 %copy-start.11 = (f32[64,2]{0,1:T(2,128)S(1)}, f32[64,2]{0,1:T(2,128)}, u32[]{:S(2)}) copy-start(f32[64,2]{0,1:T(2,128)} %param.33) | copy-start | bytes 1540
  90.4 18.6 %all-to-all-start.5 = ((bf16[2,128,256]{2,0,1:T(2,128)(2,1)}), bf16[2,128,256]{2,0,1:T(2,128)(2,1)S(1)}, u32[]{:S(2)}, u32[]{:S(2)}) async-start(bf16[2,128,256]{2,0,1:T(2,128)(2,1)} %copy.86), calls=%async_computation.5 | async-start | bytes 262144 | tf_op jit(solution)/shard_map/all_to_all | solution.py:124
where the time goes:
time: 110 us
  blocking collectives  54 us (49%)
  waiting for transfers between devices  23.4 us (21%)
  starting transfers between devices  17.3 us (16%)
  local copies, waits for them, and re-layouts  5.92 us (5%)
  matrix products  5.02 us (5%)
  other arithmetic  3.14 us (3%)
    all_to_all x1, blocking collectives, body(): lax.all_to_all(buffer, 'ep', split_axis=1, concat_axis=1, tiled=True)  41.8 us
    all_to_all x1, waiting for transfers between devices, body(): lax.all_to_all(answered, 'ep', split_axis=1, concat_axis=1, tiled=True)  12.7 us
    all_to_all x1, blocking collectives, sent_and_summed(): lax.all_to_all(pieces, axis, split_axis=0, concat_axis=0, tiled=True)  12.2 us
    all_to_all x2, starting transfers between devices, sent_to_all(): lax.all_to_all(jnp.broadcast_to(x[None], (count, *x.shape)), axis, 0, 0,...  8.15 us
    all_to_all x2, waiting for transfers between devices, sent_to_all(): lax.all_to_all(jnp.broadcast_to(x[None], (count, *x.shape)), axis, 0, 0,...  6.13 us
    all_to_all x1, starting transfers between devices, body(): lax.all_to_all(answered, 'ep', split_axis=1, concat_axis=1, tiled=True)  5.77 us
    all_to_all x1, waiting for transfers between devices, sent_and_summed(): lax.all_to_all(pieces, axis, split_axis=0, concat_axis=0, tiled=True)  4.54 us
    all_to_all x1, starting transfers between devices, sent_and_summed(): lax.all_to_all(pieces, axis, split_axis=0, concat_axis=0, tiled=True)  3.32 us
  transfers between devices with their start and end apart: 4, of which 4 were waited for; matrix products, arithmetic and copies ran while one was open for 3% of the time, Pallas kernels for 0%

commit v1 on v0

v1 whole, which is shorter than its diff:
```python
import functools

import jax
import jax.numpy as jnp
from jax import lax
from jax.experimental import pallas as pl
from jax.experimental.pallas import tpu as pltpu
from jax.sharding import PartitionSpec as P

EPS = 1e-06
LRU_SCALE = 8.0
MESH = pl.DeviceIdType.MESH
F32 = jnp.float32
BF16 = jnp.bfloat16

NX = 4
NZ = 8
NG = 16
S = 64
CAP = 2
F = 256
H = 128
ROWS = NZ * NG * CAP
D = NX * F
CH = 2
CR = ROWS // CH

RING8 = (4, 3, 5, 2, 6, 1, 7)


def remote(src, dst, send, recv, dev):
    return pltpu.make_async_remote_copy(
        src_ref=src, dst_ref=dst, send_sem=send, recv_sem=recv, device_id=dev, device_id_type=MESH
    )


def iota(shape, dim):
    return lax.broadcasted_iota(jnp.int32, shape, dim)


def dot(a, b):
    return jnp.dot(a, b, preferred_element_type=F32)


def swap_matrix(outer, inner):
    row = iota((ROWS, ROWS), 0)
    col = iota((ROWS, ROWS), 1)
    slot = lax.rem(row, CAP)
    mid = lax.rem(lax.div(row, CAP), inner)
    top = lax.div(row, CAP * inner)
    source = mid * (outer * CAP) + top * CAP + slot
    return jnp.where(col == source, 1.0, 0.0).astype(BF16)


def kernel(
    tokens,
    conv_state,
    lru_state,
    mix_gain,
    ffn_gain,
    w_branch,
    w_gate,
    conv_taps,
    w_recur,
    w_inject,
    lru_lambda,
    w_out,
    expert_gate,
    expert_up,
    expert_down,
    ids,
    weights,
    mixed_out,
    state_out,
    xg,
    conv_v,
    lru_v,
    mixg_v,
    ffng_v,
    wb_v,
    wg_v,
    taps_v,
    wr_v,
    wi_v,
    lam_v,
    wo_v,
    eg_v,
    eu_v,
    ed_v,
    ids_v,
    rw_v,
    bd,
    pick_a,
    pick_b,
    comb_a,
    comb_b,
    to_zg,
    to_gz,
    part,
    mr,
    send_a,
    send_b,
    got_a,
    got_b,
    fwd_a,
    fwd_b,
    all_a,
    all_b,
    xn,
    term_a,
    term_b,
    rel_a,
    rel_b,
    sum_a,
    sum_b,
    rs_a,
    rs_b,
    ret_a,
    ret_b,
    hop_a,
    hop_b,
    mid_a,
    mid_b,
    back_a,
    back_b,
    in_sem,
    tok_s,
    tok_r,
    mix_s,
    mix_r,
    g_s,
    g_r,
    z_s,
    z_r,
    ax_s,
    ax_r,
    bx_s,
    bx_r,
    rs_s,
    rs_r,
):
    x = lax.axis_index("tp")
    e = lax.axis_index("ep")
    z = lax.div(e, NG)
    g = lax.rem(e, NG)
    y = lax.div(g, 2)
    c = lax.rem(g, 2)

    x_dev = [(e, lax.rem(x + d, NX)) for d in range(NX)]
    x_idx = [lax.rem(x + d, NX) for d in range(NX)]
    z_peers = []
    for dz in RING8:
        i = lax.rem(z + dz, NZ)
        z_peers.append((i, (i * NG + g, x)))
    g_peers = []
    for dy in RING8 + (0,):
        for dc in (0, 1):
            if dy or dc:
                i = lax.rem(y + dy, 8) * 2 + lax.rem(c + dc, 2)
                g_peers.append((i, (z * NG + i, x)))

    barrier = pltpu.get_barrier_semaphore()
    for _, dev in z_peers + g_peers:
        pl.semaphore_signal(barrier, inc=1, device_id=dev, device_id_type=MESH)
    for dev in x_dev[1:]:
        pl.semaphore_signal(barrier, inc=1, device_id=dev, device_id_type=MESH)

    loads = {}
    pairs = (
        ("tok", tokens, xg.at[x]),
        ("ids", ids, ids_v),
        ("rw", weights, rw_v),
        ("mixg", mix_gain, mixg_v),
        ("conv", conv_state, conv_v),
        ("taps", conv_taps, taps_v),
        ("wb", w_branch, wb_v),
        ("wg", w_gate, wg_v),
        ("wr", w_recur, wr_v),
        ("wi", w_inject, wi_v),
        ("lam", lru_lambda, lam_v),
        ("lru", lru_state, lru_v),
        ("wo", w_out, wo_v),
        ("ffng", ffn_gain, ffng_v),
        ("eg", expert_gate, eg_v),
        ("eu", expert_up, eu_v),
        ("ed", expert_down, ed_v),
    )
    for i, (name, src, dst) in enumerate(pairs):
        loads[name] = pltpu.make_async_copy(src, dst, in_sem.at[i])
        loads[name].start()

    loads["tok"].wait()
    pl.semaphore_wait(barrier, len(z_peers) + len(g_peers) + NX - 1)

    sends = []

    def start(copy):
        copy.start()
        sends.append(copy)

    for d in (2, 1, 3):
        start(remote(xg.at[x], xg.at[x], tok_s.at[d], tok_r.at[x], x_dev[d]))

    loads["ids"].wait()
    loads["rw"].wait()
    for pick, comb, outer, inner in ((pick_a, comb_a, NG, NZ), (pick_b, comb_b, NZ, NG)):
        row = iota((ROWS, S), 0)
        slot = lax.rem(row, CAP).astype(F32)
        first = lax.rem(lax.div(row, CAP), inner)
        second = lax.div(row, CAP * inner)
        expert = first * NG + second if outer == NG else second * NG + first
        hit0 = jnp.where(ids_v[0:1, :] == expert, 1.0, 0.0)
        hit1 = jnp.where(ids_v[1:2, :] == expert, 1.0, 0.0)
        hit = hit0 + hit1
        earlier = jnp.where(iota((S, S), 0) < iota((S, S), 1), 1.0, 0.0).astype(BF16)
        before = dot(hit.astype(BF16), earlier)
        chosen = jnp.where(before == slot, hit, 0.0)
        pick[...] = chosen.astype(BF16)
        weight = jnp.where(before == slot, hit0 * rw_v[0:1, :] + hit1 * rw_v[1:2, :], 0.0)
        weight = jnp.transpose(weight)
        high = weight.astype(BF16)
        comb[:, 0:ROWS] = high
        comb[:, ROWS:] = (weight - high.astype(F32)).astype(BF16)
    to_zg[...] = swap_matrix(NZ, NG)
    to_gz[...] = swap_matrix(NG, NZ)

    loads["wr"].wait()
    loads["wi"].wait()
    bd[...] = jnp.zeros_like(bd)
    for h in range(2):
        lo, hi = 64 * h, 64 * h + 64
        for k, w in enumerate((wr_v, wi_v)):
            bd[lo:hi, H * k + lo : H * k + hi] = w[h]
    loads["conv"].wait()
    loads["taps"].wait()
    taps = taps_v[...].astype(F32)
    old = (
        conv_v[0].astype(F32) * taps[0:1]
        + conv_v[1].astype(F32) * taps[1:2]
        + conv_v[2].astype(F32) * taps[2:3]
    )
    loads["lam"].wait()
    decay = -LRU_SCALE * jax.nn.softplus(-lam_v[...])
    loads["lru"].wait()
    loads["mixg"].wait()
    gain = mixg_v[...].astype(F32)
    for name in ("wb", "wg", "wo"):
        loads[name].wait()

    for d in (1, 3, 2):
        remote(xg.at[x], xg.at[x_idx[d]], tok_s.at[d], tok_r.at[x_idx[d]], x_dev[d]).wait_recv()
    whole = jnp.concatenate([xg[k].astype(F32) for k in range(NX)], axis=1)
    scale = lax.rsqrt(jnp.sum(whole * whole, axis=1, keepdims=True) * (1.0 / D) + EPS)
    normed = (whole * scale * gain).astype(BF16)
    branch = dot(normed, wb_v[...]).astype(BF16)
    gate_in = dot(normed, wg_v[...]).astype(BF16).astype(F32)
    conv_out = old + branch.astype(F32) * taps[3:4]
    gates = jax.nn.sigmoid(dot(conv_out.astype(BF16), bd[...]))
    recur, inject = gates[:, :H], gates[:, H:]
    log_decay = recur * decay
    state = (
        jnp.exp(log_decay) * lru_v[...]
        + jnp.sqrt(1.0 - jnp.exp(2.0 * log_decay)) * inject * conv_out
    )
    state_out[...] = state
    lru_out = (state * jax.nn.gelu(gate_in)).astype(BF16)
    partial = dot(lru_out, wo_v[...]).astype(BF16)
    for k in range(NX):
        part[k] = partial[:, F * k : F * k + F]
    for d in (2, 1, 3):
        start(remote(part.at[x_idx[d]], mr.at[x], mix_s.at[d], mix_r.at[x], x_dev[d]))
    mix = part[x].astype(F32)
    for d in (1, 3, 2):
        remote(part.at[x], mr.at[x_idx[d]], mix_s.at[d], mix_r.at[x_idx[d]], x_dev[d]).wait_recv()
        mix = mix + mr[x_idx[d]].astype(F32)
    resid = (xg[x].astype(F32) + mix.astype(BF16).astype(F32)).astype(BF16)

    def exchange(way, peers, own, src, dst, s, r):
        for i, (p, dev) in enumerate(peers):
            start(remote(src.at[p], dst.at[own], s.at[way, i], r.at[way, own], dev))

    def arrived(way, i, p, dev, src, dst, s, r):
        remote(src.at[p], dst.at[p], s.at[way, i], r.at[way, p], dev).wait_recv()

    def all_arrived(way, peers, src, dst, s, r):
        for i, (p, dev) in reversed(list(enumerate(peers))):
            arrived(way, i, p, dev, src, dst, s, r)

    send_a[...] = dot(pick_a[...], resid[:, :H]).astype(BF16).reshape(NG, NZ * CAP, H)
    exchange(0, g_peers, g, send_a, got_a, g_s, g_r)
    send_b[...] = dot(pick_b[...], resid[:, H:]).astype(BF16).reshape(NZ, NG * CAP, H)
    exchange(0, z_peers, z, send_b, got_b, z_s, z_r)
    got_a[g] = send_a[g]
    got_b[z] = send_b[z]
    all_arrived(0, z_peers, send_b, got_b, z_s, z_r)
    fwd_b[...] = dot(to_gz[...], got_b[...].reshape(ROWS, H)).astype(BF16).reshape(NG, NZ * CAP, H)
    exchange(1, g_peers, g, fwd_b, all_b.at[x], g_s, g_r)
    all_arrived(0, g_peers, send_a, got_a, g_s, g_r)
    fwd_a[...] = dot(to_zg[...], got_a[...].reshape(ROWS, H)).astype(BF16).reshape(NZ, NG * CAP, H)
    exchange(1, z_peers, z, fwd_a, all_a.at[x], z_s, z_r)
    all_a[x, z] = fwd_a[z]
    all_b[x, g] = fwd_b[g]

    steps = (0, 1, 7, 2, 6, 3, 5, 4)
    left, right = x_idx[3], x_idx[1]

    def pass_on(j, a_src, a_to, b_src, b_to, lane):
        dz = lax.rem(z + steps[j], NZ)
        dy = lax.rem(y + steps[j], 8) * 2
        a = all_a.at[a_src, dz]
        b = all_b.at[b_src, pl.ds(dy, 2)]
        start(remote(a, a, ax_s.at[lane, j], ax_r.at[a_src, j], x_dev[a_to]))
        start(remote(b, b, bx_s.at[lane, j], bx_r.at[b_src, j], x_dev[b_to]))

    def took(src, j, a_too=True, b_too=True):
        dz = lax.rem(z + steps[j], NZ)
        dy = lax.rem(y + steps[j], 8) * 2
        if a_too:
            a = all_a.at[src, dz]
            remote(a, a, ax_s.at[0, j], ax_r.at[src, j], x_dev[1]).wait_recv()
        if b_too:
            b = all_b.at[src, pl.ds(dy, 2)]
            remote(b, b, bx_s.at[0, j], bx_r.at[src, j], x_dev[1]).wait_recv()

    def relay(j):
        took(left, j, b_too=False)
        took(right, j, a_too=False)
        pass_on(j, left, 1, right, 3, 2)

    lag = 3
    for j in range(NZ):
        if steps[j]:
            i = RING8.index(steps[j])
            p, dev = z_peers[i]
            arrived(1, i, p, dev, fwd_a, all_a.at[x], z_s, z_r)
            for i in (2 * i, 2 * i + 1):
                p, dev = g_peers[i]
                arrived(1, i, p, dev, fwd_b, all_b.at[x], g_s, g_r)
        else:
            p, dev = g_peers[14]
            arrived(1, 14, p, dev, fwd_b, all_b.at[x], g_s, g_r)
        pass_on(j, x, 1, x, 1, 0)
        pass_on(j, x, 3, x, 3, 1)
        if j >= lag:
            relay(j - lag)
    for j in range(NZ - lag, NZ):
        relay(j)
    for j in range(NZ):
        took(left, j, a_too=False)
        took(right, j, b_too=False)
    for j in range(NZ):
        took(x_idx[2], j)

    loads["ffng"].wait()
    full_b = jnp.concatenate([all_b[k].reshape(ROWS, H) for k in range(NX)], axis=1)
    full_b = dot(to_zg[...], full_b)
    pieces = []
    for k in range(NX):
        pieces.append(all_a[k].reshape(ROWS, H).astype(F32))
        pieces.append(full_b[:, H * k : H * k + H])
    rows = jnp.concatenate(pieces, axis=1)
    scale = lax.rsqrt(jnp.sum(rows * rows, axis=1, keepdims=True) * (1.0 / D) + EPS)
    xn[...] = (rows * scale * ffng_v[...].astype(F32)).astype(BF16)

    for name in ("eg", "eu", "ed"):
        loads[name].wait()

    def expert(j):
        at = slice(CR * j, CR * j + CR)
        rows = xn[at, :]
        first = dot(rows, eg_v[0])
        second = dot(rows, eu_v[0])
        hidden = (first * jax.nn.sigmoid(first) * second).astype(BF16)
        term = dot(hidden, ed_v[0]).astype(BF16)
        for k in range(NX):
            term_a[j, k] = term[:, F * k : F * k + H]
            term_b[j, k] = term[:, F * k + H : F * k + F]
        start(remote(term_a.at[j, x_idx[2]], rel_a.at[j], rs_s.at[j, 0], rs_r.at[j, 0], x_dev[1]))
        start(remote(term_b.at[j, x_idx[2]], rel_b.at[j], rs_s.at[j, 1], rs_r.at[j, 1], x_dev[3]))
        start(remote(term_b.at[j, right], rs_b.at[j, 0], rs_s.at[j, 2], rs_r.at[j, 2], x_dev[1]))
        start(remote(term_a.at[j, left], rs_a.at[j, 0], rs_s.at[j, 3], rs_r.at[j, 3], x_dev[3]))

    def landed(dst, j, lane):
        remote(dst, dst, rs_s.at[j, lane], rs_r.at[j, lane], x_dev[1]).wait_recv()

    def halfway(j):
        landed(rel_a.at[j], j, 0)
        sum_a[j] = (term_a[j, right].astype(F32) + rel_a[j].astype(F32)).astype(BF16)
        start(remote(sum_a.at[j], rs_a.at[j, 1], rs_s.at[j, 4], rs_r.at[j, 4], x_dev[1]))
        landed(rel_b.at[j], j, 1)
        sum_b[j] = (term_b[j, left].astype(F32) + rel_b[j].astype(F32)).astype(BF16)
        start(remote(sum_b.at[j], rs_b.at[j, 1], rs_s.at[j, 5], rs_r.at[j, 5], x_dev[3]))

    expert(0)
    expert(1)
    halfway(0)
    halfway(1)
    total_b = []
    for j in range(CH):
        landed(rs_a.at[j, 0], j, 3)
        landed(rs_b.at[j, 0], j, 2)
        landed(rs_a.at[j, 1], j, 4)
        landed(rs_b.at[j, 1], j, 5)
        a = term_a[j, x].astype(F32) + rs_a[j, 0].astype(F32) + rs_a[j, 1].astype(F32)
        b = term_b[j, x].astype(F32) + rs_b[j, 0].astype(F32) + rs_b[j, 1].astype(F32)
        ret_a[NZ // CH * j : NZ // CH * (j + 1)] = a.astype(BF16).reshape(NZ // CH, NG * CAP, H)
        total_b.append(b.astype(BF16))
    total_b = jnp.concatenate(total_b, axis=0)

    exchange(2, z_peers, z, ret_a, hop_a, z_s, z_r)
    ret_b[...] = dot(to_gz[...], total_b).astype(BF16).reshape(NG, NZ * CAP, H)
    exchange(2, g_peers, g, ret_b, hop_b, g_s, g_r)
    hop_a[z] = ret_a[z]
    hop_b[g] = ret_b[g]
    all_arrived(2, z_peers, ret_a, hop_a, z_s, z_r)
    mid_a[...] = dot(to_gz[...], hop_a[...].reshape(ROWS, H)).astype(BF16).reshape(NG, NZ * CAP, H)
    exchange(3, g_peers, g, mid_a, back_a, g_s, g_r)
    all_arrived(2, g_peers, ret_b, hop_b, g_s, g_r)
    mid_b[...] = dot(to_zg[...], hop_b[...].reshape(ROWS, H)).astype(BF16).reshape(NZ, NG * CAP, H)
    exchange(3, z_peers, z, mid_b, back_b, z_s, z_r)
    back_a[g] = mid_a[g]
    back_b[z] = mid_b[z]
    all_arrived(3, g_peers, mid_a, back_a, g_s, g_r)
    all_arrived(3, z_peers, mid_b, back_b, z_s, z_r)
    for half, comb, back in ((0, comb_a, back_a), (1, comb_b, back_b)):
        rows = back[...].reshape(ROWS, H)
        moe = dot(comb[:, 0:ROWS], rows) + dot(comb[:, ROWS:], rows)
        at = slice(H * half, H * half + H)
        mixed_out[:, at] = (resid[:, at].astype(F32) + moe).astype(BF16)

    for copy in sends:
        copy.wait_send()


def body(
    tokens,
    conv_state,
    lru_state,
    mix_gain,
    ffn_gain,
    w_branch,
    w_gate,
    conv_taps,
    w_recur,
    w_inject,
    lru_lambda,
    w_out,
    expert_gate,
    expert_up,
    expert_down,
    route_ids,
    route_weight,
):
    conv_state = jnp.transpose(conv_state, (1, 0, 2))
    route_ids = jnp.transpose(route_ids)
    route_weight = jnp.transpose(route_weight)
    lru_lambda = lru_lambda.reshape(1, H)
    mix_gain = mix_gain.reshape(1, D)
    ffn_gain = ffn_gain.reshape(1, D)
    operands = (
        tokens,
        conv_state,
        lru_state,
        mix_gain,
        ffn_gain,
        w_branch,
        w_gate,
        conv_taps,
        w_recur,
        w_inject,
        lru_lambda,
        w_out,
        expert_gate,
        expert_up,
        expert_down,
        route_ids,
        route_weight,
    )

    def vm(*shape, dtype=BF16):
        return pltpu.VMEM(shape, dtype)

    landing = [vm(NX, S, F)]
    landing += [pltpu.VMEM(a.shape, a.dtype) for a in operands[1:]]
    by_g = (NG, NZ * CAP, H)
    by_z = (NZ, NG * CAP, H)
    scratch = landing + [
        vm(H, 2 * H),
        vm(ROWS, S),
        vm(ROWS, S),
        vm(S, 2 * ROWS),
        vm(S, 2 * ROWS),
        vm(ROWS, ROWS),
        vm(ROWS, ROWS),
        vm(NX, S, F),
        vm(NX, S, F),
        vm(*by_g),
        vm(*by_z),
        vm(*by_g),
        vm(*by_z),
        vm(*by_z),
        vm(*by_g),
        vm(NX, *by_z),
        vm(NX, *by_g),
        vm(ROWS, D),
        vm(CH, NX, CR, H),
        vm(CH, NX, CR, H),
        vm(CH, CR, H),
        vm(CH, CR, H),
        vm(CH, CR, H),
        vm(CH, CR, H),
        vm(CH, 2, CR, H),
        vm(CH, 2, CR, H),
        vm(*by_z),
        vm(*by_g),
        vm(*by_z),
        vm(*by_g),
        vm(*by_g),
        vm(*by_z),
        vm(*by_g),
        vm(*by_z),
    ]
    dma = pltpu.SemaphoreType.DMA
    scratch += [
        dma((17,)),
        dma((NX,)),
        dma((NX,)),
        dma((NX,)),
        dma((NX,)),
        dma((4, NG)),
        dma((4, NG)),
        dma((4, NZ)),
        dma((4, NZ)),
        dma((3, NZ)),
        dma((NX, NZ)),
        dma((3, NZ)),
        dma((NX, NZ)),
        dma((CH, 6)),
        dma((CH, 6)),
    ]
    return pl.pallas_call(
        kernel,
        out_shape=(
            jax.ShapeDtypeStruct((S, F), BF16),
            jax.ShapeDtypeStruct((S, H), F32),
        ),
        in_specs=[pl.BlockSpec(memory_space=pltpu.HBM)] * len(operands),
        out_specs=(
            pl.BlockSpec(memory_space=pltpu.VMEM),
            pl.BlockSpec(memory_space=pltpu.VMEM),
        ),
        scratch_shapes=scratch,
        compiler_params=pltpu.CompilerParams(
            collective_id=0, has_side_effects=True, vmem_limit_bytes=67043328
        ),
        name="layer",
    )(*operands)


def solution(mesh):
    placed = (
        P("ep", "tp"),
        P("ep", None, "tp"),
        P("ep", "tp"),
        P(),
        P(),
        P(None, "tp"),
        P(None, "tp"),
        P(None, "tp"),
        P("tp", None, None),
        P("tp", None, None),
        P("tp"),
        P("tp", None),
        P("ep", None, "tp"),
        P("ep", None, "tp"),
        P("ep", "tp", None),
        P("ep", None),
        P("ep", None),
    )
    return jax.shard_map(
        body, mesh=mesh, in_specs=placed, out_specs=(P("ep", "tp"), P("ep", "tp")), check_vma=False
    )
```

time: 110 us -> 71.4 us (0.65)
  Pallas kernels: 0 us -> 65.2 us
  blocking collectives: 54 us -> 0 us
  waiting for transfers between devices: 23.4 us -> 0 us
  starting transfers between devices: 17.3 us -> 0 us
  matrix products: 5.02 us -> 0 us
  other arithmetic: 3.14 us -> 0 us
    pallas_call x0 -> x1, Pallas kernels: none -> 65.2 us  [body(): pl.pallas_call(kernel, out_shape=(jax.ShapeDtypeStruct((S, F), BF16), jax...]
    all_to_all x2 -> x0, blocking collectives: 54 us -> none  [the longest x1 41.8 us: body(): lax.all_to_all(buffer, 'ep', split_axis=1, concat_axis=1, tiled=True)]
    all_to_all x4 -> x0, waiting for transfers between devices: 23.4 us -> none  [the longest x1 12.7 us: body(): lax.all_to_all(answered, 'ep', split_axis=1, concat_axis=1, tiled=True)]
    all_to_all x4 -> x0, starting transfers between devices: 17.3 us -> none  [the longest x2 8.15 us: sent_to_all(): lax.all_to_all(jnp.broadcast_to(x[None], (count, *x.shape)), axis, 0, 0,...]
    dot_general x8 -> x0, matrix products: 5.02 us -> none  [the longest x1 2.39 us: body(): term = jnp.dot(hidden, expert_down[0], preferred_element_type=jnp.float32)]
    broadcast_in_dim x2 -> x0, local copies, waits for them, and re-layouts: 2.16 us -> none  [sent_to_all(): jnp.broadcast_to(x[None], (count, *x.shape))]
    unnamed x29 -> x2, local copies, waits for them, and re-layouts: 0.87 us -> 2.75 us
    convert_element_type x6 -> x0, other arithmetic: 1.47 us -> none  [the longest x2 0.69 us: rms_rows(): return (scaled * gain.astype(jnp.float32)).astype(jnp.bfloat16)]
  transfers between devices with their start and end apart: 4 -> 0, of which waited for: 4 -> 0; matrix products, arithmetic and copies ran while one was open for 3% -> 0% of each run, Pallas kernels for 0% -> 0%
where the time goes in v1:
time: 71.4 us; the launch traced here: 71.1 us
  Pallas kernels  65.2 us (91%)
  local copies, waits for them, and re-layouts  5.3 us (7%)
    pallas_call x1, Pallas kernels, body(): pl.pallas_call(kernel, out_shape=(jax.ShapeDtypeStruct((S, F), BF16), jax...  65.2 us
    unnamed x2, local copies, waits for them, and re-layouts  2.75 us

profile of v1, /device:TPU:1, one launch (start us, length us, event | category | flops | bytes accessed | tf_op | source)
XLA Modules:
  0.0 71.1 jit_solution(9015081580704855209)
XLA Ops:
  0.6 1.3 %reshape.13.mix_gain = bf16[1,1024]{1,0:T(2,128)(2,1)} reshape(bf16[1024]{0:T(1024)(128)(2,1)} %param.20) | data formatting | bytes 4096 | tf_op jit(solution)/shard_map/reshape | solution.py:458
  1.9 1.3 %reshape.14.ffn_gain = bf16[1,1024]{1,0:T(2,128)(2,1)} reshape(bf16[1024]{0:T(1024)(128)(2,1)} %param.21) | data formatting | bytes 4096 | tf_op jit(solution)/shard_map/reshape | solution.py:459
  3.2 65.2 %layer.1 = (bf16[64,256]{1,0:T(8,128)(2,1)}, f32[64,128]{1,0:T(8,128)}) custom-call(bf16[64,256]{1,0:T(8,128)(2,1)} %tokens.1, bf16[3,64,128]{2,1,0:T(8,128)(2,1)} %bitcast.4, f32[64,128]{1,0:T(8,128)} %lru_state.1, bf16[1,1024]{1,0:T(2,128)(2,1)} %reshape.13.mix_gain, bf16[1,1024]{1,0:T(2,128)(2,1)} %reshape.14.ffn_gain, bf16[1024,128]{1,0:T(8,128)(2,1)} %w_branch.1, ...), custom_call_target="tpu_custom_call" | custom-call | tf_op jit(solution)/shard_map/layer/pallas_call | solution.py:541
  68.4 1.4 %copy.21 = bf16[64,256]{1,0:T(8,128)(2,1)} copy(bf16[64,256]{1,0:T(8,128)(2,1)} %get-tuple-element.4) | data formatting | bytes 65536
  69.8 1.4 %copy.22 = f32[64,128]{1,0:T(8,128)} copy(f32[64,128]{1,0:T(8,128)} %get-tuple-element.5) | data formatting | bytes 65536

commit v2 on v1

v2 whole, which is shorter than its diff:
```python
import functools

import jax
import jax.numpy as jnp
from jax import lax
from jax.experimental import pallas as pl
from jax.experimental.pallas import tpu as pltpu
from jax.sharding import PartitionSpec as P

EPS = 1e-06
LRU_SCALE = 8.0
MESH = pl.DeviceIdType.MESH
F32 = jnp.float32
BF16 = jnp.bfloat16

NX = 4
NZ = 8
NG = 16
S = 64
CAP = 2
F = 256
H = 128
ROWS = NZ * NG * CAP
D = NX * F
HALF = ROWS // 2
EARLY = 5

RING8 = (4, 3, 5, 2, 6, 1, 7)
STEPS = (0, 1, 7, 2, 6, 3, 5, 4)


def remote(src, dst, send, recv, dev):
    return pltpu.make_async_remote_copy(
        src_ref=src, dst_ref=dst, send_sem=send, recv_sem=recv, device_id=dev, device_id_type=MESH
    )


def iota(shape, dim):
    return lax.broadcasted_iota(jnp.int32, shape, dim)


def dot(a, b):
    return jnp.dot(a, b, preferred_element_type=F32)


def swap_matrix(outer, inner):
    row = iota((ROWS, ROWS), 0)
    col = iota((ROWS, ROWS), 1)
    slot = lax.rem(row, CAP)
    mid = lax.rem(lax.div(row, CAP), inner)
    top = lax.div(row, CAP * inner)
    source = mid * (outer * CAP) + top * CAP + slot
    return jnp.where(col == source, 1.0, 0.0).astype(BF16)


def rank(offset):
    back = 2 * (8 - offset)
    return jnp.where(offset == 0, 0, jnp.where(offset <= 4, 2 * offset - 1, back))


def place_b(i, z, y):
    j = lax.div(i, NG * CAP)
    offset = jnp.where(lax.rem(j, 2) == 1, lax.div(j + 1, 2), 8 - lax.div(j, 2))
    at_z = lax.rem(z + offset, NZ)
    at_g = lax.rem(lax.div(i, CAP), NG)
    step = rank(lax.rem(lax.div(at_g, 2) + 8 - y, 8))
    return (step * 2 + lax.rem(at_g, 2)) * (NZ * CAP) + at_z * CAP + lax.rem(i, CAP)


def kernel(
    tokens,
    conv_state,
    lru_state,
    mix_gain,
    ffn_gain,
    w_branch,
    w_gate,
    conv_taps,
    w_recur,
    w_inject,
    lru_lambda,
    w_out,
    expert_gate,
    expert_up,
    expert_down,
    ids,
    weights,
    mixed_out,
    state_out,
    xg,
    conv_v,
    lru_v,
    mixg_v,
    ffng_v,
    wb_v,
    wg_v,
    taps_v,
    wr_v,
    wi_v,
    lam_v,
    wo_v,
    eg_v,
    eu_v,
    ed_v,
    ids_v,
    rw_v,
    bd,
    pick_a,
    pick_b,
    comb_a,
    comb_b,
    to_zg,
    to_gz,
    to_a,
    to_b,
    part,
    mr,
    send_a,
    send_b,
    got_a,
    got_b,
    fwd_a,
    fwd_b,
    all_a,
    all_b,
    gains,
    acc_g,
    acc_u,
    term_a,
    term_b,
    rel_a,
    rel_b,
    sum_a,
    sum_b,
    rs_a,
    rs_b,
    ret_a,
    ret_b,
    hop_a,
    hop_b,
    mid_a,
    mid_b,
    back_a,
    back_b,
    in_sem,
    x_sem,
    g_s,
    g_r,
    z_s,
    z_r,
    ax_s,
    bx_s,
    ax_step,
    bx_step,
    x_r,
    rs_s,
    rs_r,
):
    x = lax.axis_index("tp")
    e = lax.axis_index("ep")
    z = lax.div(e, NG)
    g = lax.rem(e, NG)
    y = lax.div(g, 2)
    c = lax.rem(g, 2)

    x_dev = [(e, lax.rem(x + d, NX)) for d in range(NX)]
    x_idx = [lax.rem(x + d, NX) for d in range(NX)]
    z_peers = []
    for dz in RING8:
        i = lax.rem(z + dz, NZ)
        z_peers.append((i, (i * NG + g, x)))
    g_peers = []
    for dy in RING8 + (0,):
        for dc in (0, 1):
            if dy or dc:
                i = lax.rem(y + dy, 8) * 2 + lax.rem(c + dc, 2)
                g_peers.append((i, (z * NG + i, x)))

    z_ring, g_ring = [], []
    for dy in STEPS[::-1]:
        place = STEPS.index(-dy % 8)
        if dy:
            i = lax.rem(z + dy, NZ)
            z_ring.append((place, i, (i * NG + g, x)))
        for dc in (1, 0):
            if dy or dc:
                i = lax.rem(y + dy, 8) * 2 + lax.rem(c + dc, 2)
                g_ring.append((place, i, (z * NG + i, x)))

    barrier = pltpu.get_barrier_semaphore()
    for _, dev in z_peers + g_peers:
        pl.semaphore_signal(barrier, inc=1, device_id=dev, device_id_type=MESH)
    for dev in x_dev[1:]:
        pl.semaphore_signal(barrier, inc=1, device_id=dev, device_id_type=MESH)

    loads = {}
    pairs = (
        ("tok", tokens, xg.at[x]),
        ("ids", ids, ids_v),
        ("rw", weights, rw_v),
        ("mixg", mix_gain, mixg_v),
        ("conv", conv_state, conv_v),
        ("taps", conv_taps, taps_v),
        ("wb", w_branch, wb_v),
        ("wg", w_gate, wg_v),
        ("wr", w_recur, wr_v),
        ("wi", w_inject, wi_v),
        ("lam", lru_lambda, lam_v),
        ("lru", lru_state, lru_v),
        ("wo", w_out, wo_v),
        ("ffng", ffn_gain, ffng_v),
        ("eg", expert_gate, eg_v),
        ("eu", expert_up, eu_v),
        ("ed", expert_down, ed_v),
    )
    for i, (name, src, dst) in enumerate(pairs):
        loads[name] = pltpu.make_async_copy(src, dst, in_sem.at[i])
        loads[name].start()

    loads["tok"].wait()
    pl.semaphore_wait(barrier, len(z_peers) + len(g_peers) + NX - 1)

    near = x_dev[1]

    def got(dst, sem):
        remote(dst, dst, sem, sem, near).wait_recv()

    def sent(src, sem):
        remote(src, src, sem, sem, near).wait_send()

    for d in (2, 1, 3):
        remote(xg.at[x], xg.at[x], x_sem.at[0], x_sem.at[1], x_dev[d]).start()

    loads["ids"].wait()
    loads["rw"].wait()
    for pick, comb, outer, inner in ((pick_a, comb_a, NG, NZ), (pick_b, comb_b, NZ, NG)):
        row = iota((ROWS, S), 0)
        slot = lax.rem(row, CAP).astype(F32)
        first = lax.rem(lax.div(row, CAP), inner)
        second = lax.div(row, CAP * inner)
        expert = first * NG + second if outer == NG else second * NG + first
        hit0 = jnp.where(ids_v[0:1, :] == expert, 1.0, 0.0)
        hit1 = jnp.where(ids_v[1:2, :] == expert, 1.0, 0.0)
        hit = hit0 + hit1
        earlier = jnp.where(iota((S, S), 0) < iota((S, S), 1), 1.0, 0.0).astype(BF16)
        before = dot(hit.astype(BF16), earlier)
        chosen = jnp.where(before == slot, hit, 0.0)
        pick[...] = chosen.astype(BF16)
        weight = jnp.where(before == slot, hit0 * rw_v[0:1, :] + hit1 * rw_v[1:2, :], 0.0)
        weight = jnp.transpose(weight)
        high = weight.astype(BF16)
        comb[:, 0:ROWS] = high
        comb[:, ROWS:] = (weight - high.astype(F32)).astype(BF16)
    to_zg[...] = swap_matrix(NZ, NG)
    to_gz[...] = swap_matrix(NG, NZ)
    row, col = iota((ROWS, ROWS), 0), iota((ROWS, ROWS), 1)
    to_a[...] = jnp.where(place_b(row, z, y) == col, 1.0, 0.0).astype(BF16)
    to_b[...] = jnp.where(place_b(col, z, y) == row, 1.0, 0.0).astype(BF16)

    loads["wr"].wait()
    loads["wi"].wait()
    bd[...] = jnp.zeros_like(bd)
    for h in range(2):
        lo, hi = 64 * h, 64 * h + 64
        for k, w in enumerate((wr_v, wi_v)):
            bd[lo:hi, H * k + lo : H * k + hi] = w[h]
    loads["conv"].wait()
    loads["taps"].wait()
    taps = taps_v[...].astype(F32)
    old = (
        conv_v[0].astype(F32) * taps[0:1]
        + conv_v[1].astype(F32) * taps[1:2]
        + conv_v[2].astype(F32) * taps[2:3]
    )
    loads["lam"].wait()
    decay = -LRU_SCALE * jax.nn.softplus(-lam_v[...])
    loads["lru"].wait()
    loads["mixg"].wait()
    gain = mixg_v[...].reshape(1, D).astype(F32)
    for name in ("wb", "wg", "wo"):
        loads[name].wait()

    got(xg.at[pl.ds(0, NX - 1)], x_sem.at[1])
    whole = jnp.concatenate([xg[k].astype(F32) for k in range(NX)], axis=1)
    scale = lax.rsqrt(jnp.sum(whole * whole, axis=1, keepdims=True) * (1.0 / D) + EPS)
    normed = (whole * scale * gain).astype(BF16)
    branch = dot(normed, wb_v[...]).astype(BF16)
    gate_in = dot(normed, wg_v[...]).astype(BF16).astype(F32)
    conv_out = old + branch.astype(F32) * taps[3:4]
    gates = jax.nn.sigmoid(dot(conv_out.astype(BF16), bd[...]))
    recur, inject = gates[:, :H], gates[:, H:]
    log_decay = recur * decay
    state = (
        jnp.exp(log_decay) * lru_v[...]
        + jnp.sqrt(1.0 - jnp.exp(2.0 * log_decay)) * inject * conv_out
    )
    state_out[...] = state
    lru_out = (state * jax.nn.gelu(gate_in)).astype(BF16)
    partial = dot(lru_out, wo_v[...]).astype(BF16)
    for k in range(NX):
        part[k] = partial[:, F * k : F * k + F]
    for d in (2, 1, 3):
        remote(part.at[x_idx[d]], mr.at[x], x_sem.at[2], x_sem.at[3], x_dev[d]).start()
    mix = part[x].astype(F32)
    got(mr.at[pl.ds(0, NX - 1)], x_sem.at[3])
    for d in (1, 3, 2):
        mix = mix + mr[x_idx[d]].astype(F32)
    resid = (xg[x].astype(F32) + mix.astype(BF16).astype(F32)).astype(BF16)

    def exchange(way, peers, own, src, dst, s, r):
        for p, dev in peers:
            remote(src.at[p], dst.at[own], s.at[way], r.at[way], dev).start()

    def all_arrived(way, peers, dst, r):
        got(dst.at[pl.ds(0, len(peers))], r.at[way])

    send_a[...] = dot(pick_a[...], resid[:, :H]).astype(BF16).reshape(NG, NZ * CAP, H)
    exchange(0, g_peers, g, send_a, got_a, g_s, g_r)
    send_b[...] = dot(pick_b[...], resid[:, H:]).astype(BF16).reshape(NZ, NG * CAP, H)
    exchange(0, z_peers, z, send_b, got_b, z_s, z_r)
    got_a[g] = send_a[g]
    got_b[z] = send_b[z]
    all_arrived(0, z_peers, got_b, z_r)
    fwd_b[...] = dot(to_gz[...], got_b[...].reshape(ROWS, H)).astype(BF16).reshape(NG, NZ * CAP, H)
    for j, p, dev in g_ring[::-1]:
        remote(fwd_b.at[p], all_b.at[x, 2 * j + c], g_s.at[3], g_r.at[3 + j], dev).start()
    all_arrived(0, g_peers, got_a, g_r)
    fwd_a[...] = dot(to_zg[...], got_a[...].reshape(ROWS, H)).astype(BF16).reshape(NZ, NG * CAP, H)
    for j, p, dev in z_ring[::-1]:
        remote(fwd_a.at[p], all_a.at[x, j], z_s.at[3], z_r.at[3 + j], dev).start()
    all_a[x, 0] = fwd_a[z]
    all_b[x, c] = fwd_b[g]

    left, half_way, right = x_idx[3], x_idx[2], x_idx[1]

    def pass_on(j):
        a, b = all_a.at[x, j], all_b.at[x, pl.ds(2 * j, 2)]
        if j >= EARLY:
            remote(a, a, ax_s.at[3], x_r.at[4], x_dev[2]).start()
            remote(b, b, bx_s.at[3], x_r.at[5], x_dev[2]).start()
        remote(a, a, ax_s.at[0], ax_step.at[j], x_dev[1]).start()
        remote(b, b, bx_s.at[0], bx_step.at[j], x_dev[3]).start()
        if j < 3:
            remote(a, a, ax_s.at[1], x_r.at[0], x_dev[3]).start()
            remote(b, b, bx_s.at[1], x_r.at[1], x_dev[1]).start()

    for j in range(NZ):
        if j:
            got(all_a.at[x, j], z_r.at[3 + j])
            got(all_b.at[x, pl.ds(2 * j, 2)], g_r.at[3 + j])
        else:
            got(all_b.at[x, 0], g_r.at[3])
        pass_on(j)
    a, b = all_a.at[x, pl.ds(3, NZ - 3)], all_b.at[x, pl.ds(6, 2 * NZ - 6)]
    remote(a, a, ax_s.at[1], x_r.at[0], x_dev[3]).start()
    remote(b, b, bx_s.at[1], x_r.at[1], x_dev[1]).start()
    for j in range(EARLY):
        a, b = all_a.at[left, j], all_b.at[right, pl.ds(2 * j, 2)]
        got(a, ax_step.at[j])
        remote(a, a, ax_s.at[2], x_r.at[2], x_dev[1]).start()
        got(b, bx_step.at[j])
        remote(b, b, bx_s.at[2], x_r.at[3], x_dev[3]).start()

    loads["ffng"].wait()
    gain = ffng_v[...].reshape(1, D).astype(F32)
    for k in range(NX):
        gains[k] = gain[:, F * k : F * k + F]
    for name in ("eg", "eu", "ed"):
        loads[name].wait()
    squares = jnp.zeros((ROWS, H), F32)
    for n, k in enumerate((x, left, right, half_way)):
        if n == 1:
            for j in range(EARLY, NZ):
                got(all_a.at[left, j], ax_step.at[j])
            got(all_b.at[left], x_r.at[1])
        if n == 2:
            for j in range(EARLY, NZ):
                got(all_b.at[right, pl.ds(2 * j, 2)], bx_step.at[j])
            got(all_a.at[right], x_r.at[0])
        if n == 3:
            got(all_a.at[k, pl.ds(0, EARLY)], x_r.at[2])
            got(all_b.at[k, pl.ds(0, 2 * EARLY)], x_r.at[3])
            got(all_a.at[k, pl.ds(EARLY, NZ - EARLY)], x_r.at[4])
            got(all_b.at[k, pl.ds(2 * EARLY, 2 * (NZ - EARLY))], x_r.at[5])
        a = all_a[k].reshape(ROWS, H).astype(F32)
        b = dot(to_a[...], all_b[k].reshape(ROWS, H))
        squares = squares + a * a + b * b
        rows = (jnp.concatenate([a, b], axis=1) * gains[k]).astype(BF16)
        at = pl.ds(pl.multiple_of(k * F, F), F)
        first = dot(rows, eg_v[0, at, :])
        second = dot(rows, eu_v[0, at, :])
        if n == 0:
            acc_g[...] = first
            acc_u[...] = second
        elif n < 3:
            acc_g[...] += first
            acc_u[...] += second
    scale = lax.rsqrt(jnp.sum(squares, axis=1, keepdims=True) * (1.0 / D) + EPS)
    first = (acc_g[...] + first) * scale
    second = (acc_u[...] + second) * scale
    hidden = (first * jax.nn.sigmoid(first) * second).astype(BF16)

    def down(k):
        at = pl.ds(pl.multiple_of(k * F, F), F)
        term = dot(hidden, ed_v[0, :, at]).astype(BF16)
        b = dot(to_b[...], term[:, H:]).astype(BF16)
        for j, rows in enumerate((slice(HALF, ROWS), slice(0, HALF))):
            term_a[j, k] = term[rows, :H]
            term_b[j, k] = b[rows]

    def send_term(j, src, dst, lane, dev):
        remote(src, dst, rs_s.at[j, 0], rs_r.at[j, lane], dev).start()

    down(half_way)
    for j in range(2):
        send_term(j, term_a.at[j, half_way], rel_a.at[j], 0, x_dev[1])
        send_term(j, term_b.at[j, half_way], rel_b.at[j], 1, x_dev[3])
    down(right)
    down(left)
    for j in range(2):
        send_term(j, term_b.at[j, right], rs_b.at[j, 0], 2, x_dev[1])
        send_term(j, term_a.at[j, left], rs_a.at[j, 0], 3, x_dev[3])
    down(x)

    def landed(dst, j, lane):
        got(dst, rs_r.at[j, lane])

    def halfway(j):
        landed(rel_a.at[j], j, 0)
        sum_a[j] = (term_a[j, right].astype(F32) + rel_a[j].astype(F32)).astype(BF16)
        remote(sum_a.at[j], rs_a.at[j, 1], rs_s.at[j, 1], rs_r.at[j, 4], x_dev[1]).start()
        landed(rel_b.at[j], j, 1)
        sum_b[j] = (term_b[j, left].astype(F32) + rel_b[j].astype(F32)).astype(BF16)
        remote(sum_b.at[j], rs_b.at[j, 1], rs_s.at[j, 1], rs_r.at[j, 5], x_dev[3]).start()

    halfway(0)
    halfway(1)
    for j, lo in ((0, NZ // 2), (1, 0)):
        landed(rs_a.at[j, 0], j, 3)
        landed(rs_b.at[j, 0], j, 2)
        landed(rs_a.at[j, 1], j, 4)
        landed(rs_b.at[j, 1], j, 5)
        a = term_a[j, x].astype(F32) + rs_a[j, 0].astype(F32) + rs_a[j, 1].astype(F32)
        b = term_b[j, x].astype(F32) + rs_b[j, 0].astype(F32) + rs_b[j, 1].astype(F32)
        ret_a[lo : lo + NZ // 2] = a.astype(BF16).reshape(NZ // 2, NG * CAP, H)
        ret_b[2 * lo : 2 * lo + NZ] = b.astype(BF16).reshape(NZ, NZ * CAP, H)
        for place in range(lo + NZ // 2 - 1, lo - 1, -1):
            i = lax.rem(z + STEPS[place], NZ)
            if place:
                remote(ret_a.at[place], hop_a.at[z], z_s.at[1], z_r.at[1], (i * NG + g, x)).start()
            for dc in (1, 0):
                if place or dc:
                    core = lax.rem(c + dc, 2)
                    i = lax.rem(y + STEPS[place], 8) * 2 + core
                    src = ret_b.at[2 * place + core]
                    remote(src, hop_b.at[g], g_s.at[1], g_r.at[1], (z * NG + i, x)).start()
    hop_a[z] = ret_a[0]
    hop_b[g] = ret_b[c]
    all_arrived(1, z_peers, hop_a, z_r)
    mid_a[...] = dot(to_gz[...], hop_a[...].reshape(ROWS, H)).astype(BF16).reshape(NG, NZ * CAP, H)
    exchange(2, g_peers, g, mid_a, back_a, g_s, g_r)
    all_arrived(1, g_peers, hop_b, g_r)
    mid_b[...] = dot(to_zg[...], hop_b[...].reshape(ROWS, H)).astype(BF16).reshape(NZ, NG * CAP, H)
    exchange(2, z_peers, z, mid_b, back_b, z_s, z_r)
    back_a[g] = mid_a[g]
    back_b[z] = mid_b[z]
    all_arrived(2, g_peers, back_a, g_r)
    all_arrived(2, z_peers, back_b, z_r)
    for half, comb, back in ((0, comb_a, back_a), (1, comb_b, back_b)):
        rows = back[...].reshape(ROWS, H)
        moe = dot(comb[:, 0:ROWS], rows) + dot(comb[:, ROWS:], rows)
        at = slice(H * half, H * half + H)
        mixed_out[:, at] = (resid[:, at].astype(F32) + moe).astype(BF16)

    sent(xg.at[pl.ds(0, NX - 1)], x_sem.at[0])
    sent(part.at[pl.ds(0, NX - 1)], x_sem.at[2])
    for way in range(4):
        sent(send_a.at[pl.ds(0, NG - 1)], g_s.at[way])
        sent(send_b.at[pl.ds(0, NZ - 1)], z_s.at[way])
    for lane in range(2):
        sent(all_a.at[0], ax_s.at[lane])
        sent(all_b.at[0], bx_s.at[lane])
    sent(all_a.at[0, pl.ds(0, EARLY)], ax_s.at[2])
    sent(all_b.at[0, pl.ds(0, 2 * EARLY)], bx_s.at[2])
    sent(all_a.at[0, pl.ds(EARLY, NZ - EARLY)], ax_s.at[3])
    sent(all_b.at[0, pl.ds(2 * EARLY, 2 * (NZ - EARLY))], bx_s.at[3])
    for j in range(2):
        sent(term_a.at[0], rs_s.at[j, 0])
        sent(rs_a.at[0], rs_s.at[j, 1])


def body(
    tokens,
    conv_state,
    lru_state,
    mix_gain,
    ffn_gain,
    w_branch,
    w_gate,
    conv_taps,
    w_recur,
    w_inject,
    lru_lambda,
    w_out,
    expert_gate,
    expert_up,
    expert_down,
    route_ids,
    route_weight,
):
    conv_state = jnp.transpose(conv_state, (1, 0, 2))
    route_ids = jnp.transpose(route_ids)
    route_weight = jnp.transpose(route_weight)
    lru_lambda = lru_lambda.reshape(1, H)
    operands = (
        tokens,
        conv_state,
        lru_state,
        mix_gain,
        ffn_gain,
        w_branch,
        w_gate,
        conv_taps,
        w_recur,
        w_inject,
        lru_lambda,
        w_out,
        expert_gate,
        expert_up,
        expert_down,
        route_ids,
        route_weight,
    )

    operands = tuple(pltpu.with_memory_space_constraint(a, pltpu.HBM) for a in operands)

    def vm(*shape, dtype=BF16):
        return pltpu.VMEM(shape, dtype)

    landing = [vm(NX, S, F)]
    landing += [pltpu.VMEM(a.shape, a.dtype) for a in operands[1:]]
    by_g = (NG, NZ * CAP, H)
    by_z = (NZ, NG * CAP, H)
    scratch = landing + [
        vm(H, 2 * H),
        vm(ROWS, S),
        vm(ROWS, S),
        vm(S, 2 * ROWS),
        vm(S, 2 * ROWS),
        vm(ROWS, ROWS),
        vm(ROWS, ROWS),
        vm(ROWS, ROWS),
        vm(ROWS, ROWS),
        vm(NX, S, F),
        vm(NX, S, F),
        vm(*by_g),
        vm(*by_z),
        vm(*by_g),
        vm(*by_z),
        vm(*by_z),
        vm(*by_g),
        vm(NX, *by_z),
        vm(NX, *by_g),
        vm(NX, 1, F, dtype=F32),
        vm(ROWS, expert_gate.shape[2], dtype=F32),
        vm(ROWS, expert_gate.shape[2], dtype=F32),
        vm(2, NX, HALF, H),
        vm(2, NX, HALF, H),
        vm(2, HALF, H),
        vm(2, HALF, H),
        vm(2, HALF, H),
        vm(2, HALF, H),
        vm(2, 2, HALF, H),
        vm(2, 2, HALF, H),
        vm(*by_z),
        vm(*by_g),
        vm(*by_z),
        vm(*by_g),
        vm(*by_g),
        vm(*by_z),
        vm(*by_g),
        vm(*by_z),
    ]
    dma = pltpu.SemaphoreType.DMA
    scratch += [
        dma((17,)),
        dma((4,)),
        dma((4,)),
        dma((3 + NZ,)),
        dma((4,)),
        dma((3 + NZ,)),
        dma((4,)),
        dma((4,)),
        dma((NZ,)),
        dma((NZ,)),
        dma((6,)),
        dma((2, 2)),
        dma((2, 6)),
    ]
    return pl.pallas_call(
        kernel,
        out_shape=(
            jax.ShapeDtypeStruct((S, F), BF16),
            jax.ShapeDtypeStruct((S, H), F32),
        ),
        in_specs=[pl.BlockSpec(memory_space=pltpu.HBM)] * len(operands),
        out_specs=(
            pl.BlockSpec(memory_space=pltpu.VMEM),
            pl.BlockSpec(memory_space=pltpu.VMEM),
        ),
        scratch_shapes=scratch,
        compiler_params=pltpu.CompilerParams(
            collective_id=0, has_side_effects=True, vmem_limit_bytes=33554432
        ),
        name="layer",
    )(*operands)


def solution(mesh):
    placed = (
        P("ep", "tp"),
        P("ep", None, "tp"),
        P("ep", "tp"),
        P(),
        P(),
        P(None, "tp"),
        P(None, "tp"),
        P(None, "tp"),
        P("tp", None, None),
        P("tp", None, None),
        P("tp"),
        P("tp", None),
        P("ep", None, "tp"),
        P("ep", None, "tp"),
        P("ep", "tp", None),
        P("ep", None),
        P("ep", None),
    )
    return jax.shard_map(
        body, mesh=mesh, in_specs=placed, out_specs=(P("ep", "tp"), P("ep", "tp")), check_vma=False
    )
```

time: 71.4 us -> 59.4 us (0.83)
  Pallas kernels: 65.2 us -> 57.4 us
  local copies, waits for them, and re-layouts: 5.3 us -> 1.23 us
    pallas_call x1, Pallas kernels: 65.2 us -> 57.4 us  [body(): pl.pallas_call(kernel, out_shape=(jax.ShapeDtypeStruct((S, F), BF16), jax...]
    reshape x2 -> x0, local copies, waits for them, and re-layouts: 2.56 us -> none  [the longest x1 1.28 us: body(): mix_gain = mix_gain.reshape(1, D)]
    unnamed x2, local copies, waits for them, and re-layouts: 2.75 us -> 1.23 us
where the time goes in v2:
time: 59.4 us; the launch traced here: 59.3 us
  Pallas kernels  57.4 us (97%)
  local copies, waits for them, and re-layouts  1.23 us (2%)
  between operations  0.65 us (1%)
    pallas_call x1, Pallas kernels, body(): pl.pallas_call(kernel, out_shape=(jax.ShapeDtypeStruct((S, F), BF16), jax...  57.4 us
    unnamed x2, local copies, waits for them, and re-layouts  1.23 us

profile of v2, /device:TPU:1, one launch (start us, length us, event | category | flops | bytes accessed | tf_op | source)
XLA Modules:
  0.0 59.3 jit_solution(4421154073134124973)
XLA Ops:
  0.6 57.4 %layer.1 = (bf16[64,256]{1,0:T(8,128)(2,1)S(1)}, f32[64,128]{1,0:T(8,128)S(1)}) custom-call(bf16[64,256]{1,0:T(8,128)(2,1)} %tokens.1, bf16[3,64,128]{2,1,0:T(8,128)(2,1)} %bitcast.4, f32[64,128]{1,0:T(8,128)} %lru_state.1, bf16[1024]{0:T(1024)(128)(2,1)} %mix_gain.1, bf16[1024]{0:T(1024)(128)(2,1)} %ffn_gain.1, bf16[1024,128]{1,0:T(8,128)(2,1)} %w_branch.1, ...), custom_call_target="tpu_custom_call" | custom-call | tf_op jit(solution)/shard_map/layer/pallas_call | solution.py:600
  58.1 0.6 %copy.21 = bf16[64,256]{1,0:T(8,128)(2,1)} copy(bf16[64,256]{1,0:T(8,128)(2,1)S(1)} %get-tuple-element.4) | data formatting | bytes 65536
  58.7 0.6 %copy.22 = f32[64,128]{1,0:T(8,128)} copy(f32[64,128]{1,0:T(8,128)S(1)} %get-tuple-element.5) | data formatting | bytes 65536

commit v3 on v2

--- a/solution.py
+++ b/solution.py
@@ -22,11 +22,8 @@
 H = 128
 ROWS = NZ * NG * CAP
 D = NX * F
-HALF = ROWS // 2
-EARLY = 5
 
 RING8 = (4, 3, 5, 2, 6, 1, 7)
-STEPS = (0, 1, 7, 2, 6, 3, 5, 4)
 
 
 def remote(src, dst, send, recv, dev):
@@ -51,20 +48,6 @@
     top = lax.div(row, CAP * inner)
     source = mid * (outer * CAP) + top * CAP + slot
     return jnp.where(col == source, 1.0, 0.0).astype(BF16)
-
-
-def rank(offset):
-    back = 2 * (8 - offset)
-    return jnp.where(offset == 0, 0, jnp.where(offset <= 4, 2 * offset - 1, back))
-
-
-def place_b(i, z, y):
-    j = lax.div(i, NG * CAP)
-    offset = jnp.where(lax.rem(j, 2) == 1, lax.div(j + 1, 2), 8 - lax.div(j, 2))
-    at_z = lax.rem(z + offset, NZ)
-    at_g = lax.rem(lax.div(i, CAP), NG)
-    step = rank(lax.rem(lax.div(at_g, 2) + 8 - y, 8))
-    return (step * 2 + lax.rem(at_g, 2)) * (NZ * CAP) + at_z * CAP + lax.rem(i, CAP)
 
 
 def kernel(
@@ -111,8 +94,6 @@
     comb_b,
     to_zg,
     to_gz,
-    to_a,
-    to_b,
     part,
     mr,
     send_a,
@@ -128,14 +109,6 @@
     acc_u,
     term_a,
     term_b,
-    rel_a,
-    rel_b,
-    sum_a,
-    sum_b,
-    rs_a,
-    rs_b,
-    ret_a,
-    ret_b,
     hop_a,
     hop_b,
     mid_a,
@@ -148,13 +121,8 @@
     g_r,
     z_s,
     z_r,
-    ax_s,
-    bx_s,
-    ax_step,
-    bx_step,
-    x_r,
-    rs_s,
-    rs_r,
+    shard_a,
+    shard_b,
 ):
     x = lax.axis_index("tp")
     e = lax.axis_index("ep")
@@ -175,17 +143,6 @@
             if dy or dc:
                 i = lax.rem(y + dy, 8) * 2 + lax.rem(c + dc, 2)
                 g_peers.append((i, (z * NG + i, x)))
-
-    z_ring, g_ring = [], []
-    for dy in STEPS[::-1]:
-        place = STEPS.index(-dy % 8)
-        if dy:
-            i = lax.rem(z + dy, NZ)
-            z_ring.append((place, i, (i * NG + g, x)))
-        for dc in (1, 0):
-            if dy or dc:
-                i = lax.rem(y + dy, 8) * 2 + lax.rem(c + dc, 2)
-                g_ring.append((place, i, (z * NG + i, x)))
 
     barrier = pltpu.get_barrier_semaphore()
     for _, dev in z_peers + g_peers:
@@ -253,9 +210,6 @@
         comb[:, ROWS:] = (weight - high.astype(F32)).astype(BF16)
     to_zg[...] = swap_matrix(NZ, NG)
     to_gz[...] = swap_matrix(NG, NZ)
-    row, col = iota((ROWS, ROWS), 0), iota((ROWS, ROWS), 1)
-    to_a[...] = jnp.where(place_b(row, z, y) == col, 1.0, 0.0).astype(BF16)
-    to_b[...] = jnp.where(place_b(col, z, y) == row, 1.0, 0.0).astype(BF16)
 
     loads["wr"].wait()
     loads["wi"].wait()
@@ -320,46 +274,30 @@
     exchange(0, z_peers, z, send_b, got_b, z_s, z_r)
     got_a[g] = send_a[g]
     got_b[z] = send_b[z]
+    def to_z(src, dst, s, r):
+        for dz in RING8 + (0,):
+            i = lax.rem(z + dz, NZ)
+            for d in (2, 1, 3, 0):
+                if dz or d:
+                    remote(src(d, i), dst, s, r, (i * NG + g, x_idx[d])).start()
+
+    def to_g(src, dst, s, r):
+        for dy in RING8 + (0,):
+            for dc in (1, 0):
+                i = lax.rem(y + dy, 8) * 2 + lax.rem(c + dc, 2)
+                for d in (2, 1, 3, 0):
+                    if dy or dc or d:
+                        remote(src(d, i), dst, s, r, (z * NG + i, x_idx[d])).start()
+
     all_arrived(0, z_peers, got_b, z_r)
     fwd_b[...] = dot(to_gz[...], got_b[...].reshape(ROWS, H)).astype(BF16).reshape(NG, NZ * CAP, H)
-    for j, p, dev in g_ring[::-1]:
-        remote(fwd_b.at[p], all_b.at[x, 2 * j + c], g_s.at[3], g_r.at[3 + j], dev).start()
+    to_g(lambda d, i: fwd_b.at[i], all_b.at[x, g], g_s.at[3], shard_b.at[x])
     all_arrived(0, g_peers, got_a, g_r)
     fwd_a[...] = dot(to_zg[...], got_a[...].reshape(ROWS, H)).astype(BF16).reshape(NZ, NG * CAP, H)
-    for j, p, dev in z_ring[::-1]:
-        remote(fwd_a.at[p], all_a.at[x, j], z_s.at[3], z_r.at[3 + j], dev).start()
-    all_a[x, 0] = fwd_a[z]
-    all_b[x, c] = fwd_b[g]
-
+    to_z(lambda d, i: fwd_a.at[i], all_a.at[x, z], z_s.at[3], shard_a.at[x])
+    all_a[x, z] = fwd_a[z]
+    all_b[x, g] = fwd_b[g]
     left, half_way, right = x_idx[3], x_idx[2], x_idx[1]
-
-    def pass_on(j):
-        a, b = all_a.at[x, j], all_b.at[x, pl.ds(2 * j, 2)]
-        if j >= EARLY:
-            remote(a, a, ax_s.at[3], x_r.at[4], x_dev[2]).start()
-            remote(b, b, bx_s.at[3], x_r.at[5], x_dev[2]).start()
-        remote(a, a, ax_s.at[0], ax_step.at[j], x_dev[1]).start()
-        remote(b, b, bx_s.at[0], bx_step.at[j], x_dev[3]).start()
-        if j < 3:
-            remote(a, a, ax_s.at[1], x_r.at[0], x_dev[3]).start()
-            remote(b, b, bx_s.at[1], x_r.at[1], x_dev[1]).start()
-
-    for j in range(NZ):
-        if j:
-            got(all_a.at[x, j], z_r.at[3 + j])
-            got(all_b.at[x, pl.ds(2 * j, 2)], g_r.at[3 + j])
-        else:
-            got(all_b.at[x, 0], g_r.at[3])
-        pass_on(j)
-    a, b = all_a.at[x, pl.ds(3, NZ - 3)], all_b.at[x, pl.ds(6, 2 * NZ - 6)]
-    remote(a, a, ax_s.at[1], x_r.at[0], x_dev[3]).start()
-    remote(b, b, bx_s.at[1], x_r.at[1], x_dev[1]).start()
-    for j in range(EARLY):
-        a, b = all_a.at[left, j], all_b.at[right, pl.ds(2 * j, 2)]
-        got(a, ax_step.at[j])
-        remote(a, a, ax_s.at[2], x_r.at[2], x_dev[1]).start()
-        got(b, bx_step.at[j])
-        remote(b, b, bx_s.at[2], x_r.at[3], x_dev[3]).start()
 
     loads["ffng"].wait()
     gain = ffng_v[...].reshape(1, D).astype(F32)
@@ -369,21 +307,10 @@
         loads[name].wait()
     squares = jnp.zeros((ROWS, H), F32)
     for n, k in enumerate((x, left, right, half_way)):
-        if n == 1:
-            for j in range(EARLY, NZ):
-                got(all_a.at[left, j], ax_step.at[j])
-            got(all_b.at[left], x_r.at[1])
-        if n == 2:
-            for j in range(EARLY, NZ):
-                got(all_b.at[right, pl.ds(2 * j, 2)], bx_step.at[j])
-            got(all_a.at[right], x_r.at[0])
-        if n == 3:
-            got(all_a.at[k, pl.ds(0, EARLY)], x_r.at[2])
-            got(all_b.at[k, pl.ds(0, 2 * EARLY)], x_r.at[3])
-            got(all_a.at[k, pl.ds(EARLY, NZ - EARLY)], x_r.at[4])
-            got(all_b.at[k, pl.ds(2 * EARLY, 2 * (NZ - EARLY))], x_r.at[5])
+        got(all_a.at[k] if n else all_a.at[k, pl.ds(0, NZ - 1)], shard_a.at[k])
+        got(all_b.at[k] if n else all_b.at[k, pl.ds(0, NG - 1)], shard_b.at[k])
         a = all_a[k].reshape(ROWS, H).astype(F32)
-        b = dot(to_a[...], all_b[k].reshape(ROWS, H))
+        b = dot(to_zg[...], all_b[k].reshape(ROWS, H))
         squares = squares + a * a + b * b
         rows = (jnp.concatenate([a, b], axis=1) * gains[k]).astype(BF16)
         at = pl.ds(pl.multiple_of(k * F, F), F)
@@ -400,67 +327,37 @@
     second = (acc_u[...] + second) * scale
     hidden = (first * jax.nn.sigmoid(first) * second).astype(BF16)
 
-    def down(k):
+    def down(d):
+        k = x_idx[d]
         at = pl.ds(pl.multiple_of(k * F, F), F)
         term = dot(hidden, ed_v[0, :, at]).astype(BF16)
-        b = dot(to_b[...], term[:, H:]).astype(BF16)
-        for j, rows in enumerate((slice(HALF, ROWS), slice(0, HALF))):
-            term_a[j, k] = term[rows, :H]
-            term_b[j, k] = b[rows]
-
-    def send_term(j, src, dst, lane, dev):
-        remote(src, dst, rs_s.at[j, 0], rs_r.at[j, lane], dev).start()
-
-    down(half_way)
-    for j in range(2):
-        send_term(j, term_a.at[j, half_way], rel_a.at[j], 0, x_dev[1])
-        send_term(j, term_b.at[j, half_way], rel_b.at[j], 1, x_dev[3])
-    down(right)
-    down(left)
-    for j in range(2):
-        send_term(j, term_b.at[j, right], rs_b.at[j, 0], 2, x_dev[1])
-        send_term(j, term_a.at[j, left], rs_a.at[j, 0], 3, x_dev[3])
-    down(x)
-
-    def landed(dst, j, lane):
-        got(dst, rs_r.at[j, lane])
-
-    def halfway(j):
-        landed(rel_a.at[j], j, 0)
-        sum_a[j] = (term_a[j, right].astype(F32) + rel_a[j].astype(F32)).astype(BF16)
-        remote(sum_a.at[j], rs_a.at[j, 1], rs_s.at[j, 1], rs_r.at[j, 4], x_dev[1]).start()
-        landed(rel_b.at[j], j, 1)
-        sum_b[j] = (term_b[j, left].astype(F32) + rel_b[j].astype(F32)).astype(BF16)
-        remote(sum_b.at[j], rs_b.at[j, 1], rs_s.at[j, 1], rs_r.at[j, 5], x_dev[3]).start()
-
-    halfway(0)
-    halfway(1)
-    for j, lo in ((0, NZ // 2), (1, 0)):
-        landed(rs_a.at[j, 0], j, 3)
-        landed(rs_b.at[j, 0], j, 2)
-        landed(rs_a.at[j, 1], j, 4)
-        landed(rs_b.at[j, 1], j, 5)
-        a = term_a[j, x].astype(F32) + rs_a[j, 0].astype(F32) + rs_a[j, 1].astype(F32)
-        b = term_b[j, x].astype(F32) + rs_b[j, 0].astype(F32) + rs_b[j, 1].astype(F32)
-        ret_a[lo : lo + NZ // 2] = a.astype(BF16).reshape(NZ // 2, NG * CAP, H)
-        ret_b[2 * lo : 2 * lo + NZ] = b.astype(BF16).reshape(NZ, NZ * CAP, H)
-        for place in range(lo + NZ // 2 - 1, lo - 1, -1):
-            i = lax.rem(z + STEPS[place], NZ)
-            if place:
-                remote(ret_a.at[place], hop_a.at[z], z_s.at[1], z_r.at[1], (i * NG + g, x)).start()
+        term_a[d] = term[:, :H].reshape(NZ, NG * CAP, H)
+        b = dot(to_gz[...], term[:, H:]).astype(BF16)
+        term_b[d] = b.reshape(NG, NZ * CAP, H)
+        for dy in RING8 + (0,):
+            i = lax.rem(z + dy, NZ)
+            if dy or d:
+                dev = (i * NG + g, k)
+                remote(term_a.at[d, i], hop_a.at[x * NZ + z], z_s.at[1], z_r.at[1], dev).start()
             for dc in (1, 0):
-                if place or dc:
-                    core = lax.rem(c + dc, 2)
-                    i = lax.rem(y + STEPS[place], 8) * 2 + core
-                    src = ret_b.at[2 * place + core]
-                    remote(src, hop_b.at[g], g_s.at[1], g_r.at[1], (z * NG + i, x)).start()
-    hop_a[z] = ret_a[0]
-    hop_b[g] = ret_b[c]
-    all_arrived(1, z_peers, hop_a, z_r)
-    mid_a[...] = dot(to_gz[...], hop_a[...].reshape(ROWS, H)).astype(BF16).reshape(NG, NZ * CAP, H)
+                i = lax.rem(y + dy, 8) * 2 + lax.rem(c + dc, 2)
+                if dy or dc or d:
+                    dev = (z * NG + i, k)
+                    remote(term_b.at[d, i], hop_b.at[x * NG + g], g_s.at[1], g_r.at[1], dev).start()
+
+    for d in (2, 1, 3, 0):
+        down(d)
+    hop_a[x * NZ + z] = term_a[0, z]
+    hop_b[x * NG + g] = term_b[0, g]
+    got(hop_a.at[pl.ds(0, NX * NZ - 1)], z_r.at[1])
+    a = hop_a[...].reshape(NX, ROWS, H).astype(F32)
+    a = (a[0] + a[1] + a[2] + a[3]).astype(BF16)
+    mid_a[...] = dot(to_gz[...], a).astype(BF16).reshape(NG, NZ * CAP, H)
     exchange(2, g_peers, g, mid_a, back_a, g_s, g_r)
-    all_arrived(1, g_peers, hop_b, g_r)
-    mid_b[...] = dot(to_zg[...], hop_b[...].reshape(ROWS, H)).astype(BF16).reshape(NZ, NG * CAP, H)
+    got(hop_b.at[pl.ds(0, NX * NG - 1)], g_r.at[1])
+    b = hop_b[...].reshape(NX, ROWS, H).astype(F32)
+    b = (b[0] + b[1] + b[2] + b[3]).astype(BF16)
+    mid_b[...] = dot(to_zg[...], b).astype(BF16).reshape(NZ, NG * CAP, H)
     exchange(2, z_peers, z, mid_b, back_b, z_s, z_r)
     back_a[g] = mid_a[g]
     back_b[z] = mid_b[z]
@@ -474,19 +371,12 @@
 
     sent(xg.at[pl.ds(0, NX - 1)], x_sem.at[0])
     sent(part.at[pl.ds(0, NX - 1)], x_sem.at[2])
-    for way in range(4):
+    for way in (0, 2):
         sent(send_a.at[pl.ds(0, NG - 1)], g_s.at[way])
         sent(send_b.at[pl.ds(0, NZ - 1)], z_s.at[way])
-    for lane in range(2):
-        sent(all_a.at[0], ax_s.at[lane])
-        sent(all_b.at[0], bx_s.at[lane])
-    sent(all_a.at[0, pl.ds(0, EARLY)], ax_s.at[2])
-    sent(all_b.at[0, pl.ds(0, 2 * EARLY)], bx_s.at[2])
-    sent(all_a.at[0, pl.ds(EARLY, NZ - EARLY)], ax_s.at[3])
-    sent(all_b.at[0, pl.ds(2 * EARLY, 2 * (NZ - EARLY))], bx_s.at[3])
-    for j in range(2):
-        sent(term_a.at[0], rs_s.at[j, 0])
-        sent(rs_a.at[0], rs_s.at[j, 1])
+    for way in (1, 3):
+        sent(hop_a.at[pl.ds(0, NX * NZ - 1)], z_s.at[way])
+        sent(hop_b.at[pl.ds(0, NX * NG - 1)], g_s.at[way])
 
 
 def body(
@@ -549,8 +439,6 @@
         vm(S, 2 * ROWS),
         vm(ROWS, ROWS),
         vm(ROWS, ROWS),
-        vm(ROWS, ROWS),
-        vm(ROWS, ROWS),
         vm(NX, S, F),
         vm(NX, S, F),
         vm(*by_g),
@@ -564,18 +452,10 @@
         vm(NX, 1, F, dtype=F32),
         vm(ROWS, expert_gate.shape[2], dtype=F32),
         vm(ROWS, expert_gate.shape[2], dtype=F32),
-        vm(2, NX, HALF, H),
-        vm(2, NX, HALF, H),
-        vm(2, HALF, H),
-        vm(2, HALF, H),
-        vm(2, HALF, H),
-        vm(2, HALF, H),
-        vm(2, 2, HALF, H),
-        vm(2, 2, HALF, H),
-        vm(*by_z),
-        vm(*by_g),
-        vm(*by_z),
-        vm(*by_g),
+        vm(NX, *by_z),
+        vm(NX, *by_g),
+        vm(NX * NZ, NG * CAP, H),
+        vm(NX * NG, NZ * CAP, H),
         vm(*by_g),
         vm(*by_z),
         vm(*by_g),
@@ -586,16 +466,11 @@
         dma((17,)),
         dma((4,)),
         dma((4,)),
-        dma((3 + NZ,)),
-        dma((4,)),
-        dma((3 + NZ,)),
         dma((4,)),
         dma((4,)),
-        dma((NZ,)),
-        dma((NZ,)),
-        dma((6,)),
-        dma((2, 2)),
-        dma((2, 6)),
+        dma((4,)),
+        dma((NX,)),
+        dma((NX,)),
     ]
     return pl.pallas_call(
         kernel,

time: 59.4 us -> 54.9 us (0.924)
  Pallas kernels: 57.4 us -> 52.9 us
    pallas_call x1, Pallas kernels: 57.4 us -> 52.9 us  [body(): pl.pallas_call(kernel, out_shape=(jax.ShapeDtypeStruct((S, F), BF16), jax...]
where the time goes in v3:
time: 54.9 us; the launch traced here: 54.7 us
  Pallas kernels  52.9 us (96%)
  local copies, waits for them, and re-layouts  1.23 us (2%)
  between operations  0.65 us (1%)
    pallas_call x1, Pallas kernels, body(): pl.pallas_call(kernel, out_shape=(jax.ShapeDtypeStruct((S, F), BF16), jax...  52.9 us
    unnamed x2, local copies, waits for them, and re-layouts  1.23 us

profile of v3, /device:TPU:1, one launch (start us, length us, event | category | flops | bytes accessed | tf_op | source)
XLA Modules:
  0.0 54.7 jit_solution(379289866716441060)
XLA Ops:
  0.6 52.9 %layer.1 = (bf16[64,256]{1,0:T(8,128)(2,1)S(1)}, f32[64,128]{1,0:T(8,128)S(1)}) custom-call(bf16[64,256]{1,0:T(8,128)(2,1)} %tokens.1, bf16[3,64,128]{2,1,0:T(8,128)(2,1)} %bitcast.4, f32[64,128]{1,0:T(8,128)} %lru_state.1, bf16[1024]{0:T(1024)(128)(2,1)} %mix_gain.1, bf16[1024]{0:T(1024)(128)(2,1)} %ffn_gain.1, bf16[1024,128]{1,0:T(8,128)(2,1)} %w_branch.1, ...), custom_call_target="tpu_custom_call" | custom-call | tf_op jit(solution)/shard_map/layer/pallas_call | solution.py:475
  53.5 0.6 %copy.21 = bf16[64,256]{1,0:T(8,128)(2,1)} copy(bf16[64,256]{1,0:T(8,128)(2,1)S(1)} %get-tuple-element.4) | data formatting | bytes 65536
  54.1 0.6 %copy.22 = f32[64,128]{1,0:T(8,128)} copy(f32[64,128]{1,0:T(8,128)S(1)} %get-tuple-element.5) | data formatting | bytes 65536

commit v4 on v3

--- a/solution.py
+++ b/solution.py
@@ -21,6 +21,8 @@
 F = 256
 H = 128
 ROWS = NZ * NG * CAP
+CH = 1
+CR = ROWS // CH
 D = NX * F
 
 RING8 = (4, 3, 5, 2, 6, 1, 7)
@@ -104,9 +106,8 @@
     fwd_b,
     all_a,
     all_b,
-    gains,
-    acc_g,
-    acc_u,
+    xn,
+    flat_b,
     term_a,
     term_b,
     hop_a,
@@ -275,19 +276,18 @@
     got_a[g] = send_a[g]
     got_b[z] = send_b[z]
     def to_z(src, dst, s, r):
-        for dz in RING8 + (0,):
-            i = lax.rem(z + dz, NZ)
-            for d in (2, 1, 3, 0):
+        for d in (2, 1, 3, 0):
+            for dz in RING8 + (0,):
+                i = lax.rem(z + dz, NZ)
                 if dz or d:
                     remote(src(d, i), dst, s, r, (i * NG + g, x_idx[d])).start()
 
     def to_g(src, dst, s, r):
-        for dy in RING8 + (0,):
-            for dc in (1, 0):
+        for d in (2, 1, 3, 0):
+            for dy, dc in ((dy, dc) for dy in RING8 + (0,) for dc in (1, 0)):
                 i = lax.rem(y + dy, 8) * 2 + lax.rem(c + dc, 2)
-                for d in (2, 1, 3, 0):
-                    if dy or dc or d:
-                        remote(src(d, i), dst, s, r, (z * NG + i, x_idx[d])).start()
+                if dy or dc or d:
+                    remote(src(d, i), dst, s, r, (z * NG + i, x_idx[d])).start()
 
     all_arrived(0, z_peers, got_b, z_r)
     fwd_b[...] = dot(to_gz[...], got_b[...].reshape(ROWS, H)).astype(BF16).reshape(NG, NZ * CAP, H)
@@ -297,58 +297,54 @@
     to_z(lambda d, i: fwd_a.at[i], all_a.at[x, z], z_s.at[3], shard_a.at[x])
     all_a[x, z] = fwd_a[z]
     all_b[x, g] = fwd_b[g]
-    left, half_way, right = x_idx[3], x_idx[2], x_idx[1]
 
     loads["ffng"].wait()
     gain = ffng_v[...].reshape(1, D).astype(F32)
-    for k in range(NX):
-        gains[k] = gain[:, F * k : F * k + F]
     for name in ("eg", "eu", "ed"):
         loads[name].wait()
-    squares = jnp.zeros((ROWS, H), F32)
-    for n, k in enumerate((x, left, right, half_way)):
-        got(all_a.at[k] if n else all_a.at[k, pl.ds(0, NZ - 1)], shard_a.at[k])
-        got(all_b.at[k] if n else all_b.at[k, pl.ds(0, NG - 1)], shard_b.at[k])
-        a = all_a[k].reshape(ROWS, H).astype(F32)
-        b = dot(to_zg[...], all_b[k].reshape(ROWS, H))
-        squares = squares + a * a + b * b
-        rows = (jnp.concatenate([a, b], axis=1) * gains[k]).astype(BF16)
-        at = pl.ds(pl.multiple_of(k * F, F), F)
-        first = dot(rows, eg_v[0, at, :])
-        second = dot(rows, eu_v[0, at, :])
-        if n == 0:
-            acc_g[...] = first
-            acc_u[...] = second
-        elif n < 3:
-            acc_g[...] += first
-            acc_u[...] += second
-    scale = lax.rsqrt(jnp.sum(squares, axis=1, keepdims=True) * (1.0 / D) + EPS)
-    first = (acc_g[...] + first) * scale
-    second = (acc_u[...] + second) * scale
-    hidden = (first * jax.nn.sigmoid(first) * second).astype(BF16)
-
-    def down(d):
-        k = x_idx[d]
-        at = pl.ds(pl.multiple_of(k * F, F), F)
-        term = dot(hidden, ed_v[0, :, at]).astype(BF16)
-        term_a[d] = term[:, :H].reshape(NZ, NG * CAP, H)
-        b = dot(to_gz[...], term[:, H:]).astype(BF16)
-        term_b[d] = b.reshape(NG, NZ * CAP, H)
-        for dy in RING8 + (0,):
-            i = lax.rem(z + dy, NZ)
-            if dy or d:
-                dev = (i * NG + g, k)
-                remote(term_a.at[d, i], hop_a.at[x * NZ + z], z_s.at[1], z_r.at[1], dev).start()
-            for dc in (1, 0):
-                i = lax.rem(y + dy, 8) * 2 + lax.rem(c + dc, 2)
-                if dy or dc or d:
-                    dev = (z * NG + i, k)
-                    remote(term_b.at[d, i], hop_b.at[x * NG + g], g_s.at[1], g_r.at[1], dev).start()
+    got(all_a.at[x, pl.ds(0, NZ - 1)], shard_a.at[x])
+    got(all_b.at[x, pl.ds(0, NG - 1)], shard_b.at[x])
+    for k in x_idx[1:]:
+        got(all_a.at[k], shard_a.at[k])
+        got(all_b.at[k], shard_b.at[k])
+    full_b = jnp.concatenate([all_b[k].reshape(ROWS, H) for k in range(NX)], axis=1)
+    full_b = dot(to_zg[...], full_b)
+    pieces = []
+    for k in range(NX):
+        pieces.append(all_a[k].reshape(ROWS, H).astype(F32))
+        pieces.append(full_b[:, H * k : H * k + H])
+    rows = jnp.concatenate(pieces, axis=1)
+    scale = lax.rsqrt(jnp.sum(rows * rows, axis=1, keepdims=True) * (1.0 / D) + EPS)
+    xn[...] = (rows * scale * gain).astype(BF16)
+    for j in range(CH):
+        at = slice(CR * j, CR * j + CR)
+        rows = xn[at, :]
+        first = dot(rows, eg_v[0])
+        second = dot(rows, eu_v[0])
+        hidden = (first * jax.nn.sigmoid(first) * second).astype(BF16)
+        term = dot(hidden, ed_v[0]).astype(BF16)
+        blocks = slice(NZ // CH * j, NZ // CH * (j + 1))
+        for k in range(NX):
+            term_a[k, blocks] = term[:, F * k : F * k + H].reshape(NZ // CH, NG * CAP, H)
+            flat_b[at, H * k : H * k + H] = term[:, F * k + H : F * k + F]
 
     for d in (2, 1, 3, 0):
-        down(d)
-    hop_a[x * NZ + z] = term_a[0, z]
-    hop_b[x * NG + g] = term_b[0, g]
+        for dz in RING8 + (0,):
+            i = lax.rem(z + dz, NZ)
+            if dz or d:
+                src, dev = term_a.at[x_idx[d], i], (i * NG + g, x_idx[d])
+                remote(src, hop_a.at[x * NZ + z], z_s.at[1], z_r.at[1], dev).start()
+    swapped = dot(to_gz[...], flat_b[...]).astype(BF16)
+    for k in range(NX):
+        term_b[k] = swapped[:, H * k : H * k + H].reshape(NG, NZ * CAP, H)
+    for d in (2, 1, 3, 0):
+        for dy, dc in ((dy, dc) for dy in RING8 + (0,) for dc in (1, 0)):
+            i = lax.rem(y + dy, 8) * 2 + lax.rem(c + dc, 2)
+            if dy or dc or d:
+                src, dev = term_b.at[x_idx[d], i], (z * NG + i, x_idx[d])
+                remote(src, hop_b.at[x * NG + g], g_s.at[1], g_r.at[1], dev).start()
+    hop_a[x * NZ + z] = term_a[x, z]
+    hop_b[x * NG + g] = term_b[x, g]
     got(hop_a.at[pl.ds(0, NX * NZ - 1)], z_r.at[1])
     a = hop_a[...].reshape(NX, ROWS, H).astype(F32)
     a = (a[0] + a[1] + a[2] + a[3]).astype(BF16)
@@ -449,9 +445,8 @@
         vm(*by_g),
         vm(NX, *by_z),
         vm(NX, *by_g),
-        vm(NX, 1, F, dtype=F32),
-        vm(ROWS, expert_gate.shape[2], dtype=F32),
-        vm(ROWS, expert_gate.shape[2], dtype=F32),
+        vm(ROWS, D),
+        vm(ROWS, NX * H),
         vm(NX, *by_z),
         vm(NX, *by_g),
         vm(NX * NZ, NG * CAP, H),

time: 54.9 us -> 54 us (0.984)
  Pallas kernels: 52.9 us -> 52 us
    pallas_call x1, Pallas kernels: 52.9 us -> 52 us  [body(): pl.pallas_call(kernel, out_shape=(jax.ShapeDtypeStruct((S, F), BF16), jax...]
where the time goes in v4:
time: 54 us; the launch traced here: 53.9 us
  Pallas kernels  52 us (96%)
  local copies, waits for them, and re-layouts  1.23 us (2%)
  between operations  0.65 us (1%)
    pallas_call x1, Pallas kernels, body(): pl.pallas_call(kernel, out_shape=(jax.ShapeDtypeStruct((S, F), BF16), jax...  52 us
    unnamed x2, local copies, waits for them, and re-layouts  1.23 us

profile of v4, /device:TPU:1, one launch (start us, length us, event | category | flops | bytes accessed | tf_op | source)
XLA Modules:
  0.0 53.9 jit_solution(13985696003273014129)
XLA Ops:
  0.6 52.0 %layer.1 = (bf16[64,256]{1,0:T(8,128)(2,1)S(1)}, f32[64,128]{1,0:T(8,128)S(1)}) custom-call(bf16[64,256]{1,0:T(8,128)(2,1)} %tokens.1, bf16[3,64,128]{2,1,0:T(8,128)(2,1)} %bitcast.4, f32[64,128]{1,0:T(8,128)} %lru_state.1, bf16[1024]{0:T(1024)(128)(2,1)} %mix_gain.1, bf16[1024]{0:T(1024)(128)(2,1)} %ffn_gain.1, bf16[1024,128]{1,0:T(8,128)(2,1)} %w_branch.1, ...), custom_call_target="tpu_custom_call" | custom-call | tf_op jit(solution)/shard_map/layer/pallas_call | solution.py:470
  52.6 0.6 %copy.21 = bf16[64,256]{1,0:T(8,128)(2,1)} copy(bf16[64,256]{1,0:T(8,128)(2,1)S(1)} %get-tuple-element.4) | data formatting | bytes 65536
  53.2 0.6 %copy.22 = f32[64,128]{1,0:T(8,128)} copy(f32[64,128]{1,0:T(8,128)S(1)} %get-tuple-element.5) | data formatting | bytes 65536
